TPU v7x, 32 devices: a whole 2x2x4 slice. The times are simulated.
32 devices in a mesh: ep: 16 (over z, y, x), tp: 2 (over core).
Axes of the slice: x: 2, y: 2, z: 4, core: 2. Of those that a mesh axis runs over, the one named last changes fastest.
Arguments:
- tokens: bfloat16 [256, 2048], P('ep'), may hold values from -6 to 6
- mix_gain: float32 [2048], replicated, may hold values from 0.1 to 1.9
- query_weight: bfloat16 [2048, 1024], P('ep', 'tp'), may hold values from -0.125 to 0.125
- forget_weight: bfloat16 [2048, 1024], P('ep', 'tp'), may hold values from -0.125 to 0.125
- input_weight: bfloat16 [2048, 1024], P('ep', 'tp'), may hold values from -0.125 to 0.125
- lower_bound: float32 [1024], P('tp'), may hold values from 0 to 0.9
- head_gain: float32 [1024], P('tp'), may hold values from 0.1 to 1.9
- out_weight: bfloat16 [1024, 2048], P('tp', 'ep'), may hold values from -0.1875 to 0.1875
- state: float32 [256, 8, 128, 128], P('ep', 'tp'), may hold values from -4 to 4
- ffn_gain: float32 [2048], replicated, may hold values from 0.1 to 1.9
- route_ids: int32 [256, 2], P('ep'), may hold values from 0 to 7, all different within a row; in each aligned block of 16 rows (0 to 15, 16 to 31, ...) at most 6 rows name the same one
- route_weights: float32 [256, 2], P('ep'), may hold values from 0.25 to 1
- expert_gate: bfloat16 [16, 2048, 2048], P('ep', None, 'tp'), may hold values from -0.125 to 0.125
- expert_up: bfloat16 [16, 2048, 2048], P('ep', None, 'tp'), may hold values from -0.125 to 0.125
- expert_down: bfloat16 [16, 2048, 2048], P('ep', 'tp'), may hold values from -0.09375 to 0.09375
Outputs:
- mixed_out: bfloat16 [256, 2048], P('ep', 'tp')
- new_state: float32 [256, 8, 128, 128], P('ep', 'tp')
Inputs may be any that keep to these rules, and one draw needn't show every extreme that they name: `route_ids`: each row names 2 different experts; among the rows of one device no expert is named by more than 6 rows, a bound that some block reaches of them.
All inputs are finite; a program needn't handle non-finite values.
Results may differ from a plain program's by a relative error of at most 0.015.
Values may be sent and summed in bfloat16 or wider, within the bound.
No kernel may reach another device: no remote copies, remote signals or barrier semaphores. Data moves between devices by JAX's collectives and lax.ppermute only.
A program may use at most 64 MiB of HBM per device.

v0:
```python
import functools

import jax
import jax.numpy as jnp
from jax import lax
from jax.experimental import pallas as pl
from jax.experimental.pallas import tpu as pltpu
from jax.sharding import PartitionSpec as P


EXPERTS = 8
TOP = 2
LANES = 128


epsilon = 1e-06

NEAR = (0, 1, 2, 4)
GROUP = 4


def xor_pairs(count, mask):
    return [(i, i ^ mask) for i in range(count)]


def aligned(start, size):
    return pl.ds(pl.multiple_of(start, size), size)


def call(kernel, args, outs, scratch=(), flops=3_000_000_000, traffic=100_000, mib=4, hbm=False):
    vmem = pl.BlockSpec(memory_space=pltpu.VMEM)
    return pl.pallas_call(
        kernel,
        out_shape=outs,
        in_specs=[pl.BlockSpec(memory_space=pltpu.HBM) if hbm else vmem] * len(args),
        out_specs=[vmem] * len(outs) if isinstance(outs, list) else vmem,
        scratch_shapes=list(scratch),
        compiler_params=pltpu.CompilerParams(vmem_limit_bytes=mib << 20),
        cost_estimate=pl.CostEstimate(flops=flops, bytes_accessed=traffic, transcendentals=0),
    )(*args)


def thirds(values):
    high = values.astype(jnp.bfloat16)
    rest = values - high.astype(jnp.float32)
    middle = rest.astype(jnp.bfloat16)
    low = (rest - middle.astype(jnp.float32)).astype(jnp.bfloat16)
    return high, middle, low


def spreader(count):
    shape = (3 * count, count * LANES)
    row = lax.broadcasted_iota(jnp.int32, shape, 0) % count
    col = lax.broadcasted_iota(jnp.int32, shape, 1) // LANES
    return jnp.where(row == col, 1.0, 0.0).astype(jnp.bfloat16)


def spread(values, matrix):
    return lax.dot_general(
        jnp.concatenate([part.astype(jnp.float32) for part in thirds(values)], axis=0).astype(jnp.bfloat16),
        matrix,
        (((0,), (0,)), ((), ())),
        preferred_element_type=jnp.float32,
    )


def prep_kernel(coset, tokens_ref, *refs):
    weight_refs, packed_ref, outs, sems = refs[:3], refs[3], refs[4:-1], refs[-1]
    me = lax.axis_index("ep")
    copies = []

    def start(source, target):
        copy = pltpu.make_async_copy(source, target, sems.at[len(copies)])
        copy.start()
        copies.append(copy)

    for k, ref in enumerate(weight_refs):
        size = ref.shape[1]
        start(ref, packed_ref.at[:, k * size : (k + 1) * size])
    for mask, out in zip(coset, outs):
        for k, near in enumerate(NEAR):
            block = me ^ (mask ^ near)
            start(
                tokens_ref.at[:, aligned(block * LANES, LANES)],
                out.at[:, k * LANES : (k + 1) * LANES],
            )
    for copy in copies:
        copy.wait()


def route_kernel(cap, span, ids_ref, weights_ref, info_ref, combine_ref, matrix_ref):
    matrix_ref[...] = spreader(ids_ref.shape[0])
    count = ids_ref.shape[0]
    ids, weights = ids_ref[...], weights_ref[...]
    lane = lax.broadcasted_iota(jnp.int32, (count, LANES), 1)
    picks = [ids[:, k : k + 1] == lane for k in range(TOP)]
    chosen = functools.reduce(jnp.logical_or, picks)
    earlier = lax.broadcasted_iota(jnp.int32, (count, count), 0) > lax.broadcasted_iota(
        jnp.int32, (count, count), 1
    )
    rank = jnp.dot(
        jnp.where(earlier, 1.0, 0.0).astype(jnp.bfloat16),
        jnp.where(chosen, 1.0, 0.0).astype(jnp.bfloat16),
        preferred_element_type=jnp.float32,
    )
    info_ref[...] = jnp.where(chosen, rank, 2.0 * count).astype(jnp.bfloat16)
    column = lax.broadcasted_iota(jnp.int32, combine_ref.shape, 1)
    expert = column // (span * GROUP * cap)
    place = (column % cap).astype(jnp.float32)
    total = jnp.zeros(combine_ref.shape, jnp.float32)
    for k in range(TOP):
        own = jnp.sum(jnp.where(picks[k], rank, 0.0), axis=-1, keepdims=True)
        hit = (ids[:, k : k + 1] == expert) & (own == place)
        total = total + jnp.where(hit, weights[:, k : k + 1], 0.0)
    combine_ref[...] = total


def project_kernel(group, *refs):
    token_refs, gain_ref, weight_refs, outs = (
        refs[:group],
        refs[group],
        refs[group + 1 : group + 5],
        refs[group + 5 :],
    )
    me = lax.axis_index("ep")
    rows = jnp.concatenate([ref[...] for ref in token_refs], axis=0)
    total = None
    for k, near in enumerate(NEAR):
        block = me ^ near
        gain = gain_ref[:, aligned(block * LANES, LANES)]
        scaled = (rows[:, k * LANES : (k + 1) * LANES].astype(jnp.float32) * gain).astype(jnp.bfloat16)
        term = jnp.dot(scaled, weight_refs[k][...], preferred_element_type=jnp.float32)
        total = term if total is None else total + term
    count = token_refs[0].shape[0]
    for m, out in enumerate(outs):
        out[...] = total[m * count : (m + 1) * count].astype(out.dtype)


def readout_kernel(group, outer, *refs):
    part_refs = refs[:group]
    tokens_ref, bound_ref, gain_ref, info_ref, matrix_ref, state_ref = refs[group : group + 6]
    forget_ref, fresh_ref = refs[group + 6 : group + 8]
    payloads = refs[group + 8 :]
    count = tokens_ref.shape[0]
    proj = bound_ref.shape[1]
    half = outer // 2

    tokens = tokens_ref[...].astype(jnp.float32)
    scale = lax.rsqrt(jnp.mean(tokens * tokens, axis=-1, keepdims=True) + epsilon)
    matrix = matrix_ref[...]
    for head in range(proj // LANES):

        def pick(which):
            at = slice(which * proj + head * LANES, which * proj + (head + 1) * LANES)
            total = part_refs[0][:, at].astype(jnp.float32)
            for ref in part_refs[1:]:
                total = total + ref[:, at].astype(jnp.float32)
            return total * scale

        cols = slice(head * LANES, (head + 1) * LANES)
        bound = bound_ref[:, cols]
        forget = bound + (1.0 - bound) * jax.nn.sigmoid(pick(0))
        fresh = pick(1)
        query = pick(2)
        forget_ref[:, cols] = forget
        fresh_ref[:, cols] = fresh
        kept = spread(query * forget, matrix)
        rows = [
            jnp.sum(kept[:, s * LANES : (s + 1) * LANES] * state_ref[s, head], axis=0, keepdims=True)
            for s in range(count)
        ]
        added = jnp.sum(query * (1.0 - forget), axis=-1, keepdims=True) * fresh
        readout = jnp.concatenate(rows, axis=0) + added
        normed = (
            readout
            * lax.rsqrt(jnp.mean(readout * readout, axis=-1, keepdims=True) + epsilon)
            * gain_ref[:, cols]
        ).astype(jnp.bfloat16)
        for out in payloads:
            out[:, cols] = normed

    core = lax.axis_index("tp")
    place = lax.axis_index("ep") % GROUP
    for m, out in enumerate(payloads):
        for a in range(half):
            block = (core * half + a) * GROUP + (place ^ m)
            out[:, proj + a * LANES : proj + (a + 1) * LANES] = tokens_ref[:, aligned(block * LANES, LANES)]
        out[:, proj + half * LANES :] = info_ref[...]


def update_kernel(forget_ref, fresh_ref, matrix_ref, state_ref, new_ref, slot_ref, sems):
    count = forget_ref.shape[0]
    heads = state_ref.shape[1]
    matrix = matrix_ref[...]
    copies = []
    for head in range(heads):
        cols = slice(head * LANES, (head + 1) * LANES)
        kept = spread(forget_ref[:, cols], matrix)
        fresh = fresh_ref[:, cols]
        for s in range(count):
            keep = kept[:, s * LANES : (s + 1) * LANES]
            slot_ref[head, s] = keep * state_ref[s, head] + (1.0 - keep) * fresh[s : s + 1, :]
        copy = pltpu.make_async_copy(slot_ref.at[head], new_ref.at[:, head], sems.at[head])
        copy.start()
        copies.append(copy)
    for copy in copies:
        copy.wait()


def mix_kernel(outer, *refs):
    payloads = refs[:GROUP]
    weights = refs[GROUP : GROUP + outer]
    own_ref, other_ref, resid_ref, info_ref, heads_ref, part_ref = refs[GROUP + outer :]
    me = lax.axis_index("ep")
    core = lax.axis_index("tp")
    place = me % GROUP
    line = me // GROUP
    half = outer // 2
    count = payloads[0].shape[0]
    proj = weights[0].shape[0]
    for m, ref in enumerate(payloads):
        at = aligned((place ^ m) * count, count)
        heads_ref[at, :] = ref[:, :proj]
        resid_ref[at, :] = ref[:, proj : proj + half * LANES]
        info_ref[at, :] = ref[:, proj + half * LANES :]
    heads = heads_ref[...]
    for m, ref in enumerate(weights):
        product = jnp.dot(heads, ref[...], preferred_element_type=jnp.float32)
        part_ref[:, aligned((line ^ m) * LANES, LANES)] = product.astype(jnp.bfloat16)
    size = half * LANES
    own_ref[...] = part_ref[:, aligned(core * size, size)]
    other_ref[...] = part_ref[:, aligned((1 - core) * size, size)]


def dispatch_kernel(span, own_ref, got_ref, resid_ref, info_ref, out_ref, *rest):
    backs, after_ref = rest[:-1], rest[-1]
    mixer = own_ref[...].astype(jnp.float32) + got_ref[...].astype(jnp.float32)
    after_ref[...] = (resid_ref[...].astype(jnp.float32) + mixer).astype(jnp.bfloat16)
    place = lax.axis_index("ep") % GROUP
    count = after_ref.shape[0] // GROUP
    for m, ref in enumerate(backs):
        ref[...] = after_ref[aligned((place ^ m) * count, count), :]
    after = after_ref[...]
    slots = info_ref[...].astype(jnp.float32).T
    rows = out_ref.shape[1]
    cap = rows // GROUP
    row = lax.broadcasted_iota(jnp.int32, (rows, after.shape[0]), 0)
    col = lax.broadcasted_iota(jnp.int32, (rows, after.shape[0]), 1)
    same = (row // cap) == (col // count)
    slot = (row % cap).astype(jnp.float32)
    for e in range(EXPERTS):
        chosen = same & (slots[e : e + 1, :] == slot)
        select = jnp.where(chosen, 1.0, 0.0).astype(jnp.bfloat16)
        picked = jnp.dot(select, after, preferred_element_type=jnp.float32).astype(jnp.bfloat16)
        for sp in range(span):
            out_ref[e * span + sp] = picked


def gather_rows(outer, ref, rows_ref):
    half = outer // 2
    block = ref.shape[1]
    for z in range(outer):
        for q in range(GROUP):
            for a in range(half):
                at = (a * GROUP + q) * LANES
                rows_ref[z * block : (z + 1) * block, at : at + LANES] = ref[
                    z * GROUP + q, :, a * LANES : (a + 1) * LANES
                ].astype(jnp.float32)
    return rows_ref[...]


def half_products(outer, side, ref, gain_ref, gate_ref, up_ref, rows_ref):
    width = rows_ref.shape[1]
    at = aligned(side * width, width)
    values = gather_rows(outer, ref, rows_ref)
    square = jnp.sum(values * values, axis=-1, keepdims=True)
    scaled = (values * gain_ref[:, at]).astype(jnp.bfloat16)
    gate = jnp.dot(scaled, gate_ref[0, at, :], preferred_element_type=jnp.float32)
    up = jnp.dot(scaled, up_ref[0, at, :], preferred_element_type=jnp.float32)
    return square, gate, up


def first_kernel(outer, mine_ref, gain_ref, gate_ref, up_ref, _, square_ref, gate_out, up_out, rows_ref):
    side = lax.axis_index("tp")
    square, gate, up = half_products(outer, side, mine_ref, gain_ref, gate_ref, up_ref, rows_ref)
    square_ref[...] = jnp.broadcast_to(square, square_ref.shape)
    gate_out[...] = gate
    up_out[...] = up


def pack_half(side, hidden, down_ref, out_ref, total_ref, tall_ref, block, cap):
    part = out_ref.shape[1]
    width = part * GROUP
    owners = out_ref.shape[0] // block
    total = jnp.dot(
        hidden, down_ref[0, :, aligned(side * width, width)], preferred_element_type=jnp.float32
    )
    lanes = part // LANES
    for b in range(width // LANES):
        total_ref[b] = total[:, b * LANES : (b + 1) * LANES]
    for k in range(GROUP):
        for s in range(cap):
            for b in range(lanes):
                tall_ref[b, pl.ds(k * cap + s, owners, stride=block), :] = total_ref[
                    k * lanes + b, pl.ds(s, owners, stride=cap), :
                ]
    for b in range(lanes):
        out_ref[:, b * LANES : (b + 1) * LANES] = tall_ref[b].astype(jnp.bfloat16)


def second_kernel(outer, cap, theirs_ref, gain_ref, gate_ref, up_ref, down_ref, square_ref, gate_part, up_part, hidden_ref, other_ref, rows_ref, total_ref, tall_ref):
    side = 1 - lax.axis_index("tp")
    width = 2 * rows_ref.shape[1]
    square, gate, up = half_products(outer, side, theirs_ref, gain_ref, gate_ref, up_ref, rows_ref)
    scale = lax.rsqrt((square_ref[:, :1] + square) / width + epsilon)
    gate = (gate_part[...] + gate) * scale
    up = (up_part[...] + up) * scale
    hidden = (jax.nn.silu(gate) * up).astype(jnp.bfloat16)
    hidden_ref[...] = hidden
    pack_half(side, hidden, down_ref, other_ref, total_ref, tall_ref, GROUP * cap, cap)


def third_kernel(cap, hidden_ref, down_ref, own_ref, total_ref, tall_ref):
    side = lax.axis_index("tp")
    pack_half(side, hidden_ref[...], down_ref, own_ref, total_ref, tall_ref, GROUP * cap, cap)


def combine_kernel(outer, cap, got_ref, weight_ref, *refs):
    afters, out_ref, base_ref = refs[:GROUP], refs[GROUP], refs[GROUP + 1]
    place = lax.axis_index("ep") % GROUP
    half = outer // 2
    for m, ref in enumerate(afters):
        for a in range(half):
            at = (a * GROUP + (place ^ m)) * LANES
            base_ref[:, aligned(at, LANES)] = ref[:, a * LANES : (a + 1) * LANES].astype(jnp.float32)
    weight = weight_ref[...]
    values = got_ref[...]
    _, part = values.shape
    block = GROUP * cap
    count = weight.shape[0]
    piece = (lax.broadcasted_iota(jnp.int32, weight.shape, 1) % block) // cap
    parts = thirds(weight)
    for k in range(GROUP):
        split = [jnp.where(piece == k, w.astype(jnp.float32), 0.0) for w in parts]
        stacked = jnp.concatenate(split, axis=0).astype(jnp.bfloat16)
        mix = jnp.dot(stacked, values, preferred_element_type=jnp.float32)
        mix = mix[:count] + mix[count : 2 * count] + mix[2 * count :]
        at = slice(k * part, (k + 1) * part)
        out_ref[:, at] = (base_ref[:, at] + mix).astype(jnp.bfloat16)


def fast_shards(
    tokens,
    mix_gain,
    query_weight,
    forget_weight,
    input_weight,
    lower_bound,
    head_gain,
    out_weight,
    state,
    ffn_gain,
    route_ids,
    route_weights,
    expert_gate,
    expert_up,
    expert_down,
):
    bf16, f32 = jnp.bfloat16, jnp.float32
    ep = lax.axis_size("ep")
    count, width = tokens.shape
    heads, size = state.shape[1], state.shape[2]
    proj = query_weight.shape[1]
    outer = ep // GROUP
    half = outer // 2
    span = ep // EXPERTS
    coset = [h * 8 + b for h in range(ep // 8) for b in (0, 7)]

    def move(value, mask):
        if not mask:
            return value
        return lax.ppermute(value, "ep", xor_pairs(ep, mask))

    def swap(value):
        return lax.ppermute(value, "tp", [(0, 1), (1, 0)])

    def shaped(*shape, dtype=bf16):
        return jax.ShapeDtypeStruct(shape, dtype)

    packed, *sent = call(
        functools.partial(prep_kernel, coset),
        [pltpu.with_memory_space_constraint(a, pltpu.HBM) for a in (tokens, forget_weight, input_weight, query_weight)],
        [shaped(LANES, 3 * proj)] + [shaped(count, len(NEAR) * LANES)] * len(coset),
        scratch=[pltpu.SemaphoreType.DMA((3 + len(coset) * len(NEAR),))],
        hbm=True,
    )
    weights = [move(packed, near) for near in NEAR]
    token_blocks = [move(value, mask) for value, mask in zip(sent, coset)]
    out_weights = [move(out_weight, GROUP * m) for m in range(outer)]

    cap = 3 * count // 8
    rows_out = GROUP * cap
    info, combine, matrix = call(
        functools.partial(route_kernel, cap, span),
        (route_ids, route_weights),
        [shaped(count, LANES), shaped(count, ep * rows_out, dtype=f32), shaped(3 * count, count * LANES)],
    )

    parts = call(
        functools.partial(project_kernel, len(coset)),
        (*token_blocks, mix_gain.reshape(1, width), *weights),
        [shaped(count, 3 * proj)] * len(coset),
    )
    parts = [move(value, mask) for value, mask in zip(parts, coset)]

    pay = proj + half * LANES + LANES
    args = (
        *parts,
        tokens,
        lower_bound.reshape(1, proj),
        head_gain.reshape(1, proj),
        info,
        matrix,
        state,
    )
    forget, fresh, *payloads = call(
        functools.partial(readout_kernel, len(coset), outer),
        args,
        [shaped(count, proj, dtype=f32)] * 2 + [shaped(count, pay)] * GROUP,
    )
    payloads = [move(value, m) for m, value in enumerate(payloads)]
    vmem = pl.BlockSpec(memory_space=pltpu.VMEM)
    new_state = pl.pallas_call(
        update_kernel,
        out_shape=shaped(*state.shape, dtype=f32),
        in_specs=[vmem] * 4,
        out_specs=pl.BlockSpec(memory_space=pltpu.HBM),
        scratch_shapes=[
            pltpu.VMEM((heads, count, size, size), f32),
            pltpu.SemaphoreType.DMA((heads,)),
        ],
        compiler_params=pltpu.CompilerParams(vmem_limit_bytes=12 << 20),
        cost_estimate=pl.CostEstimate(flops=1_000_000_000, bytes_accessed=100_000, transcendentals=0),
    )(forget, fresh, matrix, state)

    tall = GROUP * count
    own, other, resid, infos = call(
        functools.partial(mix_kernel, outer),
        (*payloads, *out_weights),
        [shaped(tall, half * LANES)] * 3 + [shaped(tall, LANES)],
        scratch=[pltpu.VMEM((tall, proj), bf16), pltpu.VMEM((tall, outer * LANES), bf16)],
    )
    got = swap(other)
    outgoing, *afters = call(
        functools.partial(dispatch_kernel, span),
        (own, got, resid, infos),
        [shaped(ep, rows_out, half * LANES)] + [shaped(count, half * LANES)] * GROUP,
        scratch=[pltpu.VMEM((tall, half * LANES), bf16)],
    )
    slot_rows = lax.all_to_all(outgoing, "ep", split_axis=0, concat_axis=0, tiled=True)
    afters = [move(value, m) for m, value in enumerate(afters)]
    other_rows = swap(slot_rows)

    total_rows = ep * cap
    tall = ep * rows_out
    part = width // 2 // GROUP
    wide = expert_gate.shape[2]
    gain = ffn_gain.reshape(1, width)
    rows_scratch = [pltpu.VMEM((total_rows, width // 2), f32)]
    pack_scratch = [
        pltpu.VMEM((width // 2 // LANES, total_rows, LANES), f32),
        pltpu.VMEM((part // LANES, tall, LANES), f32),
    ]
    square, gate_part, up_part = call(
        functools.partial(first_kernel, outer),
        (slot_rows, gain, expert_gate, expert_up, expert_down),
        [shaped(total_rows, LANES, dtype=f32)] + [shaped(total_rows, wide, dtype=f32)] * 2,
        scratch=rows_scratch,
        mib=14,
        flops=100_000_000,
    )
    hidden, theirs = call(
        functools.partial(second_kernel, outer, cap),
        (other_rows, gain, expert_gate, expert_up, expert_down, square, gate_part, up_part),
        [shaped(total_rows, wide), shaped(tall, part)],
        scratch=rows_scratch + pack_scratch,
        mib=20,
    )
    theirs = swap(theirs)
    mine = call(
        functools.partial(third_kernel, cap),
        (hidden, expert_down),
        [shaped(tall, part)],
        scratch=pack_scratch,
        mib=10,
    )[0]
    reduced = (mine.astype(f32) + theirs.astype(f32)).astype(bf16)
    returned = lax.all_to_all(
        reduced.reshape(ep, rows_out, part), "ep", split_axis=0, concat_axis=0, tiled=True
    )
    mixed_out = call(
        functools.partial(combine_kernel, outer, cap),
        (returned.reshape(tall, part), combine, *afters),
        shaped(count, width // 2),
        scratch=[pltpu.VMEM((count, width // 2), f32)],
    )
    return (mixed_out, new_state)


def rms_scale(values_in, gain_vec):
    return (
        values_in
        * lax.rsqrt(jnp.mean(values_in * values_in, axis=-1, keepdims=True) + epsilon)
        * gain_vec
    )


def slot_ranks(block_ids, expert_count):
    onehot = (block_ids[..., None] == jnp.arange(expert_count, dtype=jnp.int32)).astype(jnp.int32)
    before = jnp.cumsum(onehot, axis=1) - onehot
    return jnp.sum(before * onehot, axis=-1)


def general_shards(
    tokens,
    mix_gain,
    query_weight,
    forget_weight,
    input_weight,
    lower_bound,
    head_gain,
    out_weight,
    state,
    ffn_gain,
    route_ids,
    route_weights,
    expert_gate,
    expert_up,
    expert_down,
):
    seq_dev = tokens.shape[0]
    model_width = tokens.shape[1]
    ep_count = lax.axis_size("ep")
    residual = tokens.astype(jnp.float32)
    normed = rms_scale(residual, mix_gain).astype(jnp.bfloat16)
    head_count = state.shape[1]
    head_size = state.shape[2]
    proj_width = query_weight.shape[1]
    pieces = (
        lax.all_gather(query_weight, "ep", axis=0, tiled=True),
        lax.all_gather(forget_weight, "ep", axis=0, tiled=True),
        lax.all_gather(input_weight, "ep", axis=0, tiled=True),
    )
    queries, forget_pre, fresh_values = tuple(
        (jnp.dot(normed, weight_rows, preferred_element_type=jnp.float32) for weight_rows in pieces)
    )
    forget = (lower_bound + (1.0 - lower_bound) * jax.nn.sigmoid(forget_pre)).reshape(
        seq_dev, head_count, head_size
    )
    queries = queries.reshape(seq_dev, head_count, head_size)
    fresh_values = fresh_values.reshape(seq_dev, head_count, head_size)
    new_state = forget[..., None] * state + (1.0 - forget)[..., None] * fresh_values[:, :, None, :]
    readout = jnp.einsum("shk,shkv->shv", queries, new_state, precision=lax.Precision.HIGHEST)
    readout = rms_scale(readout, head_gain.reshape(head_count, head_size))
    heads_out = readout.reshape(seq_dev, proj_width).astype(jnp.bfloat16)
    partial_mix = jnp.dot(
        heads_out,
        lax.all_gather(out_weight, "ep", axis=1, tiled=True),
        preferred_element_type=jnp.float32,
    )
    mixer_sum = lax.psum(partial_mix.astype(jnp.bfloat16), "tp").astype(jnp.float32)
    after_mixer = (residual + mixer_sum).astype(jnp.bfloat16)
    ffn_in = rms_scale(after_mixer.astype(jnp.float32), ffn_gain).astype(jnp.bfloat16)
    capacity = 3 * seq_dev // 8
    expert_span = ep_count // EXPERTS
    half_width = model_width // lax.axis_size("tp")
    own_columns = lax.dynamic_slice_in_dim(
        after_mixer, lax.axis_index("tp") * half_width, half_width, 1
    ).astype(jnp.float32)
    gate_slice = expert_gate[0]
    up_slice = expert_up[0]
    down_slice = expert_down[0]
    slot_iota = jnp.arange(capacity, dtype=jnp.int32)
    own_rank = slot_ranks(route_ids.reshape(1, seq_dev * TOP), EXPERTS).reshape(seq_dev, TOP)
    expert_iota = jnp.arange(EXPERTS, dtype=jnp.int32)
    chosen = (route_ids[:, :, None, None] == expert_iota[None, None, :, None]) & (
        own_rank[:, :, None, None] == slot_iota[None, None, None, :]
    )
    dispatch = jnp.any(chosen, axis=1).astype(jnp.bfloat16)
    combine = jnp.sum(chosen.astype(jnp.float32) * route_weights[:, :, None, None], axis=1)
    outgoing = jnp.einsum(
        "tec,td->ecd", dispatch, ffn_in, preferred_element_type=jnp.float32
    ).astype(jnp.bfloat16)
    outgoing = jnp.broadcast_to(
        outgoing[:, None], (EXPERTS, expert_span, capacity, model_width)
    ).reshape(ep_count, capacity, model_width)
    slot_rows = lax.all_to_all(outgoing, "ep", split_axis=0, concat_axis=0, tiled=True)
    gate_pre = jnp.einsum(
        "...d,df->...f", slot_rows, gate_slice, preferred_element_type=jnp.float32
    )
    up_pre = jnp.einsum("...d,df->...f", slot_rows, up_slice, preferred_element_type=jnp.float32)
    hidden = (jax.nn.silu(gate_pre) * up_pre).astype(jnp.bfloat16)
    partial_out = jnp.einsum(
        "...f,fd->...d", hidden, down_slice, preferred_element_type=jnp.float32
    )
    reduced = lax.psum_scatter(
        partial_out.astype(jnp.bfloat16), "tp", scatter_dimension=2, tiled=True
    ).astype(jnp.float32)
    returned = lax.all_to_all(
        reduced.astype(jnp.bfloat16), "ep", split_axis=0, concat_axis=0, tiled=True
    ).astype(reduced.dtype)
    expert_out = jnp.sum(returned.reshape(EXPERTS, expert_span, capacity, half_width), axis=1)
    expert_mix = jnp.einsum("tec,ecd->td", combine, expert_out, precision=lax.Precision.HIGHEST)
    mixed_out = (own_columns + expert_mix).astype(jnp.bfloat16)
    return (mixed_out, new_state)


def shards(*args):
    tokens, query_weight, state = args[0], args[2], args[8]
    ep, tp = lax.axis_size("ep"), lax.axis_size("tp")
    fits = (
        tp == 2
        and ep % 8 == 0
        and ep % EXPERTS == 0
        and tokens.shape[0] % 16 == 0
        and 3 * tokens.shape[0] // 8 % 2 == 0
        and tokens.shape[1] == ep * LANES
        and query_weight.shape[0] == LANES
        and state.shape[2:] == (LANES, LANES)
        and args[12].shape[2] % (4 * LANES) == 0
    )
    if not fits:
        return general_shards(*args)
    return fast_shards(*args)


def solution(mesh):
    return jax.shard_map(
        shards,
        mesh=mesh,
        in_specs=(
            P("ep", None),
            P(),
            P("ep", "tp"),
            P("ep", "tp"),
            P("ep", "tp"),
            P("tp"),
            P("tp"),
            P("tp", "ep"),
            P("ep", "tp", None, None),
            P(),
            P("ep", None),
            P("ep", None),
            P("ep", None, "tp"),
            P("ep", None, "tp"),
            P("ep", "tp", None),
        ),
        out_specs=(P("ep", "tp"), P("ep", "tp", None, None)),
        check_vma=False,
    )
```

profile of v0, /device:TPU:0, one launch (start us, length us, event | category | flops | bytes accessed | tf_op | source)
XLA Modules:
  0.0 78.1 jit_solution(1138116399677062609)
XLA Ops:
  0.6 0.0 copy-start.11
  0.6 0.0 copy-start.12
  0.7 0.0 copy-start.6
  0.7 0.0 copy-start.8
  0.7 1.3 %shard_map.158 = (bf16[128,1536]{1,0:T(8,128)(2,1)S(1)}, bf16[16,512]{1,0:T(8,128)(2,1)S(1)}, bf16[16,512]{1,0:T(8,128)(2,1)S(1)}, bf16[16,512]{1,0:T(8,128)(2,1)S(1)}, bf16[16,512]{1,0:T(8,128)(2,1)S(1)}) custom-call(bf16[16,2048]{1,0:T(8,128)(2,1)} %refs_4_.2, bf16[128,512]{1,0:T(8,128)(2,1)} %refs_0_.1, bf16[128,512]{1,0:T(8,128)(2,1)} %refs_1_.1, ...), custom_call_target="tpu_custom_call" | custom-call | flops 3000000000 | bytes 100000 | tf_op jit(solution)/shard_map/pallas_call | solution.py:32
  1.9 3.1 %collective-permute-start.5 = (bf16[128,1536]{1,0:T(8,128)(2,1)S(1)}, bf16[128,1536]{1,0:T(8,128)(2,1)S(1)}, u32[]{:S(2)}, u32[]{:S(2)}) collective-permute-start(bf16[128,1536]{1,0:T(8,128)(2,1)S(1)} %get-tuple-element.38.refs_5_), channel_id=1, source_target_pairs={{0,8},{2,10},{4,12},{6,14},{8,0},{10,2},{12,4},{14,6},{16,24},{18,... | collective-permute-start | bytes 1179656 | tf_op jit(solution)/shard_map/ppermute | solution.py:382
  5.1 1.5 %collective-permute-start.4 = (bf16[128,1536]{1,0:T(8,128)(2,1)S(1)}, bf16[128,1536]{1,0:T(8,128)(2,1)S(1)}, u32[]{:S(2)}, u32[]{:S(2)}) collective-permute-start(bf16[128,1536]{1,0:T(8,128)(2,1)S(1)} %get-tuple-element.38.refs_5_), channel_id=1, source_target_pairs={{0,4},{2,6},{4,0},{6,2},{8,12},{10,14},{12,8},{14,10},{16,20},{18,... | collective-permute-start | bytes 1179656 | tf_op jit(solution)/shard_map/ppermute | solution.py:382
  6.6 1.5 %collective-permute-start.3 = (bf16[128,1536]{1,0:T(8,128)(2,1)S(1)}, bf16[128,1536]{1,0:T(8,128)(2,1)S(1)}, u32[]{:S(2)}, u32[]{:S(2)}) collective-permute-start(bf16[128,1536]{1,0:T(8,128)(2,1)S(1)} %get-tuple-element.38.refs_5_), channel_id=1, source_target_pairs={{0,2},{2,0},{4,6},{6,4},{8,10},{10,8},{12,14},{14,12},{16,18},{18,... | collective-permute-start | bytes 1179656 | tf_op jit(solution)/shard_map/ppermute | solution.py:382
  8.1 0.0 collective-permute-start
  8.1 2.9 %collective-permute-start.1 = (bf16[16,512]{1,0:T(8,128)(2,1)S(1)}, bf16[16,512]{1,0:T(8,128)(2,1)S(1)}, u32[]{:S(2)}, u32[]{:S(2)}) collective-permute-start(bf16[16,512]{1,0:T(8,128)(2,1)S(1)} %get-tuple-element.36), channel_id=1, source_target_pairs={{0,16},{2,18},{4,20},{6,22},{8,24},{10,26},{12,28},{14,30},{16,0},... | collective-permute-start | bytes 49160 | tf_op jit(solution)/shard_map/ppermute | solution.py:382
  11.0 6.0 %collective-permute-done.refs_1_ = bf16[16,512]{1,0:T(8,128)(2,1)S(1)} collective-permute-done((bf16[16,512]{1,0:T(8,128)(2,1)S(1)}, bf16[16,512]{1,0:T(8,128)(2,1)S(1)}, u32[]{:S(2)}, u32[]{:S(2)}) %collective-permute-start) | collective-permute-done | bytes 16416 | tf_op jit(solution)/shard_map/ppermute | solution.py:382
  17.0 3.5 %collective-permute-start.2 = (bf16[16,512]{1,0:T(8,128)(2,1)S(1)}, bf16[16,512]{1,0:T(8,128)(2,1)S(1)}, u32[]{:S(2)}, u32[]{:S(2)}) collective-permute-start(bf16[16,512]{1,0:T(8,128)(2,1)S(1)} %get-tuple-element.37), channel_id=1, source_target_pairs={{0,30},{2,28},{4,26},{6,24},{8,22},{10,20},{12,18},{14,16},{16,14}... | collective-permute-start | bytes 49160 | tf_op jit(solution)/shard_map/ppermute | solution.py:382
  20.6 0.1 copy.17.ids_ref
  20.6 0.1 copy.18.weights_ref
  20.7 0.0 collective-permute-done.1.refs_2_
  20.7 0.0 collective-permute-start.13
  20.8 3.9 %collective-permute-done.2.refs_3_ = bf16[16,512]{1,0:T(8,128)(2,1)S(1)} collective-permute-done((bf16[16,512]{1,0:T(8,128)(2,1)S(1)}, bf16[16,512]{1,0:T(8,128)(2,1)S(1)}, u32[]{:S(2)}, u32[]{:S(2)}) %collective-permute-start.2) | collective-permute-done | bytes 16416 | tf_op jit(solution)/shard_map/ppermute | solution.py:382
  24.6 0.8 %collective-permute-start.12 = (bf16[512,128]{1,0:T(8,128)(2,1)S(1)}, bf16[512,128]{1,0:T(8,128)(2,1)S(1)}, u32[]{:S(2)}, u32[]{:S(2)}) collective-permute-start(bf16[512,128]{1,0:T(8,128)(2,1)S(1)} %copy-done.6), channel_id=1, source_target_pairs={{0,8},{2,10},{4,12},{6,14},{8,0},{10,2},{12,4},{14,6},{16,24},{18,... | collective-permute-start | bytes 393224 | tf_op jit(solution)/shard_map/ppermute | solution.py:382
  25.5 0.0 collective-permute-done.5.refs_8_
  25.5 0.0 collective-permute-done.4.refs_7_
  25.5 0.0 collective-permute-done.3.refs_6_
  25.5 0.4 shard_map.159
  25.9 1.0 %collective-permute-start.6 = (bf16[16,1536]{1,0:T(8,128)(2,1)S(1)}, bf16[16,1536]{1,0:T(8,128)(2,1)S(1)}, u32[]{:S(2)}, u32[]{:S(2)}) collective-permute-start(bf16[16,1536]{1,0:T(8,128)(2,1)S(1)} %get-tuple-element.40), channel_id=1, source_target_pairs={{0,14},{2,12},{4,10},{6,8},{8,6},{10,4},{12,2},{14,0},{16,30},{18,... | collective-permute-start | bytes 147464 | tf_op jit(solution)/shard_map/ppermute | solution.py:382
  26.9 2.3 %collective-permute-start.7 = (bf16[16,1536]{1,0:T(8,128)(2,1)S(1)}, bf16[16,1536]{1,0:T(8,128)(2,1)S(1)}, u32[]{:S(2)}, u32[]{:S(2)}) collective-permute-start(bf16[16,1536]{1,0:T(8,128)(2,1)S(1)} %get-tuple-element.41), channel_id=1, source_target_pairs={{0,16},{2,18},{4,20},{6,22},{8,24},{10,26},{12,28},{14,30},{16,0},... | collective-permute-start | bytes 147464 | tf_op jit(solution)/shard_map/ppermute | solution.py:382
  29.2 3.3 %collective-permute-start.8 = (bf16[16,1536]{1,0:T(8,128)(2,1)S(1)}, bf16[16,1536]{1,0:T(8,128)(2,1)S(1)}, u32[]{:S(2)}, u32[]{:S(2)}) collective-permute-start(bf16[16,1536]{1,0:T(8,128)(2,1)S(1)} %get-tuple-element.42), channel_id=1, source_target_pairs={{0,30},{2,28},{4,26},{6,24},{8,22},{10,20},{12,18},{14,16},{16,14}... | collective-permute-start | bytes 147464 | tf_op jit(solution)/shard_map/ppermute | solution.py:382
  32.4 0.3 shard_map.160
  32.7 0.0 collective-permute-done.6.refs_1_
  32.7 2.4 %collective-permute-start.14 = (bf16[512,128]{1,0:T(8,128)(2,1)S(1)}, bf16[512,128]{1,0:T(8,128)(2,1)S(1)}, u32[]{:S(2)}, u32[]{:S(2)}) collective-permute-start(bf16[512,128]{1,0:T(8,128)(2,1)S(1)} %copy-done.6), channel_id=1, source_target_pairs={{0,24},{2,26},{4,28},{6,30},{8,16},{10,18},{12,20},{14,22},{16,8},... | collective-permute-start | bytes 393224 | tf_op jit(solution)/shard_map/ppermute | solution.py:382
  35.1 0.0 collective-permute-done.7.refs_2_
  35.1 1.8 %collective-permute-done.8.refs_3_ = bf16[16,1536]{1,0:T(8,128)(2,1)S(1)} collective-permute-done((bf16[16,1536]{1,0:T(8,128)(2,1)S(1)}, bf16[16,1536]{1,0:T(8,128)(2,1)S(1)}, u32[]{:S(2)}, u32[]{:S(2)}) %collective-permute-start.8) | collective-permute-done | bytes 49184 | tf_op jit(solution)/shard_map/ppermute | solution.py:382
  37.0 1.0 %shard_map.161 = (f32[16,512]{1,0:T(8,128)S(1)}, f32[16,512]{1,0:T(8,128)S(1)}, bf16[16,896]{1,0:T(8,128)(2,1)S(1)}, bf16[16,896]{1,0:T(8,128)(2,1)S(1)}, bf16[1...) custom-call(bf16[16,1536]{1,0:T(8,128)(2,1)S(1)} %get-tuple-element.39.refs_0_, ...), custom_call_target="tpu_custom_call" | custom-call | flops 3000000000 | bytes 100000 | tf_op jit(solution)/shard_map/pallas_call | solution.py:32
  37.9 1.4 %collective-permute-start.9 = (bf16[16,896]{1,0:T(8,128)(2,1)S(1)}, bf16[16,896]{1,0:T(8,128)(2,1)S(1)}, u32[]{:S(2)}, u32[]{:S(2)}) collective-permute-start(bf16[16,896]{1,0:T(8,128)(2,1)S(1)} %get-tuple-element.46), channel_id=1, source_target_pairs={{0,2},{2,0},{4,6},{6,4},{8,10},{10,8},{12,14},{14,12},{16,18},{18,... | collective-permute-start | bytes 86024 | tf_op jit(solution)/shard_map/ppermute | solution.py:382
  39.4 1.5 %collective-permute-start.10 = (bf16[16,896]{1,0:T(8,128)(2,1)S(1)}, bf16[16,896]{1,0:T(8,128)(2,1)S(1)}, u32[]{:S(2)}, u32[]{:S(2)}) collective-permute-start(bf16[16,896]{1,0:T(8,128)(2,1)S(1)} %get-tuple-element.47), channel_id=1, source_target_pairs={{0,4},{2,6},{4,0},{6,2},{8,12},{10,14},{12,8},{14,10},{16,20},{18,... | collective-permute-start | bytes 86024 | tf_op jit(solution)/shard_map/ppermute | solution.py:382
  40.9 0.0 collective-permute-done.13.refs_6_
  40.9 0.6 collective-permute-start.11
  41.4 0.0 collective-permute-done.12.refs_5_
  41.4 0.0 collective-permute-done.14.refs_7_
  41.4 0.4 collective-permute-done.9.refs_1_
  41.8 1.4 %collective-permute-done.10.refs_2_ = bf16[16,896]{1,0:T(8,128)(2,1)S(1)} collective-permute-done((bf16[16,896]{1,0:T(8,128)(2,1)S(1)}, bf16[16,896]{1,0:T(8,128)(2,1)S(1)}, u32[]{:S(2)}, u32[]{:S(2)}) %collective-permute-start.10) | collective-permute-done | bytes 28704 | tf_op jit(solution)/shard_map/ppermute | solution.py:382
  43.2 2.4 %collective-permute-done.11.refs_3_ = bf16[16,896]{1,0:T(8,128)(2,1)S(1)} collective-permute-done((bf16[16,896]{1,0:T(8,128)(2,1)S(1)}, bf16[16,896]{1,0:T(8,128)(2,1)S(1)}, u32[]{:S(2)}, u32[]{:S(2)}) %collective-permute-start.11) | collective-permute-done | bytes 28704 | tf_op jit(solution)/shard_map/ppermute | solution.py:382
  45.6 0.2 shard_map.162
  45.9 0.1 collective-permute-start.15
  45.9 1.2 %collective-permute-done.15.got_ref = bf16[64,256]{1,0:T(8,128)(2,1)S(1)} collective-permute-done((bf16[64,256]{1,0:T(8,128)(2,1)S(1)}, bf16[64,256]{1,0:T(8,128)(2,1)S(1)}, u32[]{:S(2)}, u32[]{:S(2)}) %collective-permute-start.15) | collective-permute-done | bytes 32800 | tf_op jit(solution)/shard_map/ppermute | solution.py:385
  47.2 0.2 shard_map.163
  47.4 12.4 %all_to_all.10.mine_ref = bf16[16,24,256]{2,1,0:T(8,128)(2,1)S(1)} all-to-all(bf16[16,24,256]{2,1,0:T(8,128)(2,1)S(1)} %get-tuple-element.53), channel_id=1, replica_groups=mesh['ep'=16,'tp'=2] {'ep'}, dimensions={0} | all-to-all | bytes 393216 | tf_op jit(solution)/shard_map/all_to_all | solution.py:460
  59.8 0.0 collective-permute-start.16
  59.8 0.8 %shard_map.164 = (f32[96,128]{1,0:T(8,128)S(1)}, f32[96,1024]{1,0:T(8,128)S(1)}, f32[96,1024]{1,0:T(8,128)S(1)}) custom-call(bf16[16,24,256]{2,1,0:T(8,128)(2,1)S(1)} %all_to_all.10.mine_ref, f32[1,2048]{1,0:T(1,128)S(1)} %bitcast.7, bf16[1,2048,1024]{2,1,0:T(8,128)(2,1)S(1)} %copy-done, bf16[1,2048,1024]{2,1,0:T(8,128)(2,1)S(1)} %copy-done.1, ...), custom_call_target="tpu_custom_call" | custom-call | flops 100000000 | bytes 100000 | tf_op jit(solution)/shard_map/pallas_call | solution.py:32
  60.7 0.6 collective-permute-done.16.theirs_ref
  61.3 1.3 %shard_map.165 = (bf16[96,1024]{1,0:T(8,128)(2,1)S(1)}, bf16[384,256]{1,0:T(8,128)(2,1)S(1)}) custom-call(bf16[16,24,256]{2,1,0:T(8,128)(2,1)S(1)} %collective-permute-done.16.theirs_ref, f32[1,2048]{1,0:T(1,128)S(1)} %bitcast.8, bf16[1,2048,1024]{2,1,0:T(8,128)(2,1)S(1)} %copy-done, bf16[1,2048,1024]{2,1,0:T(8,128)(2,1)S(1)} %copy-done.1, ...), custom_call_target="tpu_custom_call" | custom-call | flops 3000000000 | bytes 100000 | tf_op jit(solution)/shard_map/pallas_call | solution.py:32
  62.6 0.2 collective-permute-start.17
  62.8 0.5 shard_map.166
  63.3 0.8 collective-permute-done.17
  64.1 0.7 add_convert_fusion
  64.8 3.5 %all-to-all-start.1 = ((bf16[16,24,256]{2,1,0:T(8,128)(2,1)}), bf16[16,24,256]{2,1,0:T(8,128)(2,1)S(1)}, u32[]{:S(2)}, u32[]{:S(2)}) async-start(bf16[16,24,256]{2,1,0:T(8,128)(2,1)} %bitcast.4), calls=%async_computation.1 | async-start | bytes 393216 | tf_op jit(solution)/shard_map/all_to_all | solution.py:498
  68.3 1.8 %collective-permute-start.18 = (bf16[16,256]{1,0:T(8,128)(2,1)S(1)}, bf16[16,256]{1,0:T(8,128)(2,1)S(1)}, u32[]{:S(2)}, u32[]{:S(2)}) collective-permute-start(bf16[16,256]{1,0:T(8,128)(2,1)S(1)} %get-tuple-element.61), channel_id=1, source_target_pairs={{0,2},{2,0},{4,6},{6,4},{8,10},{10,8},{12,14},{14,12},{16,18},{18,... | collective-permute-start | bytes 24584 | tf_op jit(solution)/shard_map/ppermute | solution.py:382
  70.1 1.5 %collective-permute-start.19 = (bf16[16,256]{1,0:T(8,128)(2,1)S(1)}, bf16[16,256]{1,0:T(8,128)(2,1)S(1)}, u32[]{:S(2)}, u32[]{:S(2)}) collective-permute-start(bf16[16,256]{1,0:T(8,128)(2,1)S(1)} %get-tuple-element.62), channel_id=1, source_target_pairs={{0,4},{2,6},{4,0},{6,2},{8,12},{10,14},{12,8},{14,10},{16,20},{18,... | collective-permute-start | bytes 24584 | tf_op jit(solution)/shard_map/ppermute | solution.py:382
  71.6 0.3 collective-permute-start.20
  71.9 2.2 %copy-done.4 = f32[16,4,128,128]{3,2,1,0:T(8,128)S(1)} copy-done((f32[16,4,128,128]{3,2,1,0:T(8,128)S(1)}, f32[16,4,128,128]{3,2,1,0:T(8,128)}, u32[]{:S(2)}) %copy-start.4) | copy-done | bytes 4194328
  74.1 2.4 %shard_map.168 = f32[16,4,128,128]{3,2,1,0:T(8,128)} custom-call(f32[16,512]{1,0:T(8,128)S(1)} %get-tuple-element.64.forget_ref, f32[16,512]{1,0:T(8,128)S(1)} %get-tuple-element.65.fresh_ref, bf16[48,2048]{1,0:T(8,128)(2,1)S(1)} %get-tuple-element.44.refs_8_.matrix_ref, f32[16,4,128,128]{3,2,1,0:T(8,128)S(1)} %copy-done.4), custom_call_target="tpu_custom_call" | custom-call | flops 1000000000 | bytes 100000 | tf_op jit(solution)/shard_map/pallas_call | solution.py:433
  76.5 0.0 collective-permute-done.18.refs_1_
  76.5 0.0 collective-permute-done.19.refs_2_
  76.5 0.0 collective-permute-done.20.refs_3_
  76.5 0.7 all-to-all-done.1
  77.2 0.9 %shard_map.167 = bf16[16,1024]{1,0:T(8,128)(2,1)} custom-call(bf16[384,256]{1,0:T(8,128)(2,1)S(1)} %bitcast.6, f32[16,384]{1,0:T(8,128)S(1)} %get-tuple-element.59.weight_ref, bf16[16,256]{1,0:T(8,128)(2,1)S(1)} %get-tuple-element.60.refs_0_, bf16[16,256]{1,0:T(8,128)(2,1)S(1)} %collective-permute-done.18.refs_1_, ...), custom_call_target="tpu_custom_call" | custom-call | flops 3000000000 | bytes 100000 | tf_op jit(solution)/shard_map/pallas_call | solution.py:32
  (21 shorter events, 0.0 us)
Async XLA Ops:
  0.6 19.9 %copy-start.11 = (s32[16,2]{0,1:T(2,128)S(1)}, s32[16,2]{0,1:T(2,128)}, u32[]{:S(2)}) copy-start(s32[16,2]{0,1:T(2,128)} %param.25) | copy-start | bytes 388
  0.6 20.0 %copy-start.12 = (f32[16,2]{0,1:T(2,128)S(1)}, f32[16,2]{0,1:T(2,128)}, u32[]{:S(2)}) copy-start(f32[16,2]{0,1:T(2,128)} %param.26) | copy-start | bytes 388
  0.7 20.1 %copy-start.6 = (bf16[512,128]{1,0:T(8,128)(2,1)S(1)}, bf16[512,128]{1,0:T(8,128)(2,1)}, u32[]{:S(2)}) copy-start(bf16[512,128]{1,0:T(8,128)(2,1)} %refs_4_.3) | copy-start | bytes 393220
  0.7 24.8 %copy-start.8 = (f32[2048]{0:T(1024)S(1)}, f32[2048]{0:T(1024)}, u32[]{:S(2)}) copy-start(f32[2048]{0:T(1024)} %param.16) | copy-start | bytes 24580
  1.9 23.5 %collective-permute-start.5 = (bf16[128,1536]{1,0:T(8,128)(2,1)S(1)}, bf16[128,1536]{1,0:T(8,128)(2,1)S(1)}, u32[]{:S(2)}, u32[]{:S(2)}) collective-permute-start(bf16[128,1536]{1,0:T(8,128)(2,1)S(1)} %get-tuple-element.38.refs_5_), channel_id=1, source_target_pairs={{0,8},{2,10},{4,12},{6,14},{8,0},{10,2},{12,4},{14,6},{16,24},{18,... | collective-permute-start | bytes 1179656 | tf_op jit(solution)/shard_map/ppermute | solution.py:382
  5.1 20.4 %collective-permute-start.4 = (bf16[128,1536]{1,0:T(8,128)(2,1)S(1)}, bf16[128,1536]{1,0:T(8,128)(2,1)S(1)}, u32[]{:S(2)}, u32[]{:S(2)}) collective-permute-start(bf16[128,1536]{1,0:T(8,128)(2,1)S(1)} %get-tuple-element.38.refs_5_), channel_id=1, source_target_pairs={{0,4},{2,6},{4,0},{6,2},{8,12},{10,14},{12,8},{14,10},{16,20},{18,... | collective-permute-start | bytes 1179656 | tf_op jit(solution)/shard_map/ppermute | solution.py:382
  6.6 18.9 %collective-permute-start.3 = (bf16[128,1536]{1,0:T(8,128)(2,1)S(1)}, bf16[128,1536]{1,0:T(8,128)(2,1)S(1)}, u32[]{:S(2)}, u32[]{:S(2)}) collective-permute-start(bf16[128,1536]{1,0:T(8,128)(2,1)S(1)} %get-tuple-element.38.refs_5_), channel_id=1, source_target_pairs={{0,2},{2,0},{4,6},{6,4},{8,10},{10,8},{12,14},{14,12},{16,18},{18,... | collective-permute-start | bytes 1179656 | tf_op jit(solution)/shard_map/ppermute | solution.py:382
  8.1 9.0 %collective-permute-start = (bf16[16,512]{1,0:T(8,128)(2,1)S(1)}, bf16[16,512]{1,0:T(8,128)(2,1)S(1)}, u32[]{:S(2)}, u32[]{:S(2)}) collective-permute-start(bf16[16,512]{1,0:T(8,128)(2,1)S(1)} %get-tuple-element.35), channel_id=1, source_target_pairs={{0,14},{2,12},{4,10},{6,8},{8,6},{10,4},{12,2},{14,0},{16,30},{18,... | collective-permute-start | bytes 49160 | tf_op jit(solution)/shard_map/ppermute | solution.py:382
  8.1 12.6 %collective-permute-start.1 = (bf16[16,512]{1,0:T(8,128)(2,1)S(1)}, bf16[16,512]{1,0:T(8,128)(2,1)S(1)}, u32[]{:S(2)}, u32[]{:S(2)}) collective-permute-start(bf16[16,512]{1,0:T(8,128)(2,1)S(1)} %get-tuple-element.36), channel_id=1, source_target_pairs={{0,16},{2,18},{4,20},{6,22},{8,24},{10,26},{12,28},{14,30},{16,0},... | collective-permute-start | bytes 49160 | tf_op jit(solution)/shard_map/ppermute | solution.py:382
  17.0 7.6 %collective-permute-start.2 = (bf16[16,512]{1,0:T(8,128)(2,1)S(1)}, bf16[16,512]{1,0:T(8,128)(2,1)S(1)}, u32[]{:S(2)}, u32[]{:S(2)}) collective-permute-start(bf16[16,512]{1,0:T(8,128)(2,1)S(1)} %get-tuple-element.37), channel_id=1, source_target_pairs={{0,30},{2,28},{4,26},{6,24},{8,22},{10,20},{12,18},{14,16},{16,14}... | collective-permute-start | bytes 49160 | tf_op jit(solution)/shard_map/ppermute | solution.py:382
  20.7 20.1 %collective-permute-start.13 = (bf16[512,128]{1,0:T(8,128)(2,1)S(1)}, bf16[512,128]{1,0:T(8,128)(2,1)S(1)}, u32[]{:S(2)}, u32[]{:S(2)}) collective-permute-start(bf16[512,128]{1,0:T(8,128)(2,1)S(1)} %copy-done.6), channel_id=1, source_target_pairs={{0,16},{2,18},{4,20},{6,22},{8,24},{10,26},{12,28},{14,30},{16,0},... | collective-permute-start | bytes 393224 | tf_op jit(solution)/shard_map/ppermute | solution.py:382
  24.6 16.8 %collective-permute-start.12 = (bf16[512,128]{1,0:T(8,128)(2,1)S(1)}, bf16[512,128]{1,0:T(8,128)(2,1)S(1)}, u32[]{:S(2)}, u32[]{:S(2)}) collective-permute-start(bf16[512,128]{1,0:T(8,128)(2,1)S(1)} %copy-done.6), channel_id=1, source_target_pairs={{0,8},{2,10},{4,12},{6,14},{8,0},{10,2},{12,4},{14,6},{16,24},{18,... | collective-permute-start | bytes 393224 | tf_op jit(solution)/shard_map/ppermute | solution.py:382
  25.9 6.8 %collective-permute-start.6 = (bf16[16,1536]{1,0:T(8,128)(2,1)S(1)}, bf16[16,1536]{1,0:T(8,128)(2,1)S(1)}, u32[]{:S(2)}, u32[]{:S(2)}) collective-permute-start(bf16[16,1536]{1,0:T(8,128)(2,1)S(1)} %get-tuple-element.40), channel_id=1, source_target_pairs={{0,14},{2,12},{4,10},{6,8},{8,6},{10,4},{12,2},{14,0},{16,30},{18,... | collective-permute-start | bytes 147464 | tf_op jit(solution)/shard_map/ppermute | solution.py:382
  26.9 8.3 %collective-permute-start.7 = (bf16[16,1536]{1,0:T(8,128)(2,1)S(1)}, bf16[16,1536]{1,0:T(8,128)(2,1)S(1)}, u32[]{:S(2)}, u32[]{:S(2)}) collective-permute-start(bf16[16,1536]{1,0:T(8,128)(2,1)S(1)} %get-tuple-element.41), channel_id=1, source_target_pairs={{0,16},{2,18},{4,20},{6,22},{8,24},{10,26},{12,28},{14,30},{16,0},... | collective-permute-start | bytes 147464 | tf_op jit(solution)/shard_map/ppermute | solution.py:382
  29.1 7.8 %copy-start.3 = (f32[16,4,128,128]{3,2,1,0:T(8,128)S(1)}, f32[16,4,128,128]{3,2,1,0:T(8,128)}, u32[]{:S(2)}) copy-start(f32[16,4,128,128]{3,2,1,0:T(8,128)} %state_ref.1) | copy-start | bytes 12582916
  29.1 7.8 %copy-start.7 = (bf16[16,2048]{1,0:T(8,128)(2,1)S(1)}, bf16[16,2048]{1,0:T(8,128)(2,1)}, u32[]{:S(2)}) copy-start(bf16[16,2048]{1,0:T(8,128)(2,1)} %refs_4_.2) | copy-start | bytes 196612
  29.1 7.8 %copy-start.9 = (f32[512]{0:T(512)S(1)}, f32[512]{0:T(512)}, u32[]{:S(2)}) copy-start(f32[512]{0:T(512)} %param.20) | copy-start | bytes 6148
  29.1 7.8 %copy-start.10 = (f32[512]{0:T(512)S(1)}, f32[512]{0:T(512)}, u32[]{:S(2)}) copy-start(f32[512]{0:T(512)} %param.21) | copy-start | bytes 6148
  29.2 7.8 %collective-permute-start.8 = (bf16[16,1536]{1,0:T(8,128)(2,1)S(1)}, bf16[16,1536]{1,0:T(8,128)(2,1)S(1)}, u32[]{:S(2)}, u32[]{:S(2)}) collective-permute-start(bf16[16,1536]{1,0:T(8,128)(2,1)S(1)} %get-tuple-element.42), channel_id=1, source_target_pairs={{0,30},{2,28},{4,26},{6,24},{8,22},{10,20},{12,18},{14,16},{16,14}... | collective-permute-start | bytes 147464 | tf_op jit(solution)/shard_map/ppermute | solution.py:382
  32.7 8.7 %collective-permute-start.14 = (bf16[512,128]{1,0:T(8,128)(2,1)S(1)}, bf16[512,128]{1,0:T(8,128)(2,1)S(1)}, u32[]{:S(2)}, u32[]{:S(2)}) collective-permute-start(bf16[512,128]{1,0:T(8,128)(2,1)S(1)} %copy-done.6), channel_id=1, source_target_pairs={{0,24},{2,26},{4,28},{6,30},{8,16},{10,18},{12,20},{14,22},{16,8},... | collective-permute-start | bytes 393224 | tf_op jit(solution)/shard_map/ppermute | solution.py:382
  37.9 3.9 %collective-permute-start.9 = (bf16[16,896]{1,0:T(8,128)(2,1)S(1)}, bf16[16,896]{1,0:T(8,128)(2,1)S(1)}, u32[]{:S(2)}, u32[]{:S(2)}) collective-permute-start(bf16[16,896]{1,0:T(8,128)(2,1)S(1)} %get-tuple-element.46), channel_id=1, source_target_pairs={{0,2},{2,0},{4,6},{6,4},{8,10},{10,8},{12,14},{14,12},{16,18},{18,... | collective-permute-start | bytes 86024 | tf_op jit(solution)/shard_map/ppermute | solution.py:382
  39.4 3.9 %collective-permute-start.10 = (bf16[16,896]{1,0:T(8,128)(2,1)S(1)}, bf16[16,896]{1,0:T(8,128)(2,1)S(1)}, u32[]{:S(2)}, u32[]{:S(2)}) collective-permute-start(bf16[16,896]{1,0:T(8,128)(2,1)S(1)} %get-tuple-element.47), channel_id=1, source_target_pairs={{0,4},{2,6},{4,0},{6,2},{8,12},{10,14},{12,8},{14,10},{16,20},{18,... | collective-permute-start | bytes 86024 | tf_op jit(solution)/shard_map/ppermute | solution.py:382
  40.9 4.8 %collective-permute-start.11 = (bf16[16,896]{1,0:T(8,128)(2,1)S(1)}, bf16[16,896]{1,0:T(8,128)(2,1)S(1)}, u32[]{:S(2)}, u32[]{:S(2)}) collective-permute-start(bf16[16,896]{1,0:T(8,128)(2,1)S(1)} %get-tuple-element.48), channel_id=1, source_target_pairs={{0,6},{2,4},{4,2},{6,0},{8,14},{10,12},{12,10},{14,8},{16,22},{18,... | collective-permute-start | bytes 86024 | tf_op jit(solution)/shard_map/ppermute | solution.py:382
  45.6 14.2 %copy-start.2 = (bf16[1,1024,2048]{2,1,0:T(8,128)(2,1)S(1)}, bf16[1,1024,2048]{2,1,0:T(8,128)(2,1)}, u32[]{:S(2)}) copy-start(bf16[1,1024,2048]{2,1,0:T(8,128)(2,1)} %down_ref.3) | copy-start | bytes 12582916
  45.9 1.3 %collective-permute-start.15 = (bf16[64,256]{1,0:T(8,128)(2,1)S(1)}, bf16[64,256]{1,0:T(8,128)(2,1)S(1)}, u32[]{:S(2)}, u32[]{:S(2)}) collective-permute-start(bf16[64,256]{1,0:T(8,128)(2,1)S(1)} %get-tuple-element.50), channel_id=1, source_target_pairs={{0,1},{1,0},{2,3},{3,2},{4,5},{5,4},{6,7},{7,6},{8,9},{9,8},{10,11... | collective-permute-start | bytes 98312 | tf_op jit(solution)/shard_map/ppermute | solution.py:385
  47.1 12.7 %copy-start = (bf16[1,2048,1024]{2,1,0:T(8,128)(2,1)S(1)}, bf16[1,2048,1024]{2,1,0:T(8,128)(2,1)}, u32[]{:S(2)}) copy-start(bf16[1,2048,1024]{2,1,0:T(8,128)(2,1)} %gate_ref.3) | copy-start | bytes 12582916
  47.1 12.7 %copy-start.1 = (bf16[1,2048,1024]{2,1,0:T(8,128)(2,1)S(1)}, bf16[1,2048,1024]{2,1,0:T(8,128)(2,1)}, u32[]{:S(2)}) copy-start(bf16[1,2048,1024]{2,1,0:T(8,128)(2,1)} %up_ref.3) | copy-start | bytes 12582916
  47.1 12.7 %copy-start.5 = (f32[2048]{0:T(1024)S(1)}, f32[2048]{0:T(1024)}, u32[]{:S(2)}) copy-start(f32[2048]{0:T(1024)} %param.24) | copy-start | bytes 24580
  59.8 1.4 %collective-permute-start.16 = (bf16[16,24,256]{2,1,0:T(8,128)(2,1)S(1)}, bf16[16,24,256]{2,1,0:T(8,128)(2,1)S(1)}, u32[]{:S(2)}, u32[]{:S(2)}) collective-permute-start(bf16[16,24,256]{2,1,0:T(8,128)(2,1)S(1)} %all_to_all.10.mine_ref), channel_id=1, source_target_pairs={{0,1},{1,0},{2,3},{3,2},{4,5},{5,4},{6,7},{7,6},{8,9},{9,8},{10,11... | collective-permute-start | bytes 589832 | tf_op jit(solution)/shard_map/ppermute | solution.py:385
  62.6 1.5 %collective-permute-start.17 = (bf16[384,256]{1,0:T(8,128)(2,1)S(1)}, bf16[384,256]{1,0:T(8,128)(2,1)S(1)}, u32[]{:S(2)}, u32[]{:S(2)}) collective-permute-start(bf16[384,256]{1,0:T(8,128)(2,1)S(1)} %get-tuple-element.58), channel_id=1, source_target_pairs={{0,1},{1,0},{2,3},{3,2},{4,5},{5,4},{6,7},{7,6},{8,9},{9,8},{10,11... | collective-permute-start | bytes 589832 | tf_op jit(solution)/shard_map/ppermute | solution.py:385
  64.8 12.4 %all-to-all-start.1 = ((bf16[16,24,256]{2,1,0:T(8,128)(2,1)}), bf16[16,24,256]{2,1,0:T(8,128)(2,1)S(1)}, u32[]{:S(2)}, u32[]{:S(2)}) async-start(bf16[16,24,256]{2,1,0:T(8,128)(2,1)} %bitcast.4), calls=%async_computation.1 | async-start | bytes 393216 | tf_op jit(solution)/shard_map/all_to_all | solution.py:498
  68.3 8.1 %collective-permute-start.18 = (bf16[16,256]{1,0:T(8,128)(2,1)S(1)}, bf16[16,256]{1,0:T(8,128)(2,1)S(1)}, u32[]{:S(2)}, u32[]{:S(2)}) collective-permute-start(bf16[16,256]{1,0:T(8,128)(2,1)S(1)} %get-tuple-element.61), channel_id=1, source_target_pairs={{0,2},{2,0},{4,6},{6,4},{8,10},{10,8},{12,14},{14,12},{16,18},{18,... | collective-permute-start | bytes 24584 | tf_op jit(solution)/shard_map/ppermute | solution.py:382
  70.1 6.3 %collective-permute-start.19 = (bf16[16,256]{1,0:T(8,128)(2,1)S(1)}, bf16[16,256]{1,0:T(8,128)(2,1)S(1)}, u32[]{:S(2)}, u32[]{:S(2)}) collective-permute-start(bf16[16,256]{1,0:T(8,128)(2,1)S(1)} %get-tuple-element.62), channel_id=1, source_target_pairs={{0,4},{2,6},{4,0},{6,2},{8,12},{10,14},{12,8},{14,10},{16,20},{18,... | collective-permute-start | bytes 24584 | tf_op jit(solution)/shard_map/ppermute | solution.py:382
  71.6 4.9 %collective-permute-start.20 = (bf16[16,256]{1,0:T(8,128)(2,1)S(1)}, bf16[16,256]{1,0:T(8,128)(2,1)S(1)}, u32[]{:S(2)}, u32[]{:S(2)}) collective-permute-start(bf16[16,256]{1,0:T(8,128)(2,1)S(1)} %get-tuple-element.63), channel_id=1, source_target_pairs={{0,6},{2,4},{4,2},{6,0},{8,14},{10,12},{12,10},{14,8},{16,22},{18,... | collective-permute-start | bytes 24584 | tf_op jit(solution)/shard_map/ppermute | solution.py:382
  71.9 2.2 %copy-start.4 = (f32[16,4,128,128]{3,2,1,0:T(8,128)S(1)}, f32[16,4,128,128]{3,2,1,0:T(8,128)}, u32[]{:S(2)}) copy-start(f32[16,4,128,128]{3,2,1,0:T(8,128)} %state_ref.1) | copy-start | bytes 12582916
where the time goes:
time: 78.4 us; the launch traced here: 78.1 us
  starting transfers between devices  33.3 us (42%)
  waiting for transfers between devices  19.2 us (24%)
  blocking collectives  12.4 us (16%)
  Pallas kernels  9.21 us (12%)
  local copies, waits for them, and re-layouts  2.4 us (3%)
  between operations  0.86 us (1%)
    ppermute x18, starting transfers between devices, move(): return lax.ppermute(value, 'ep', xor_pairs(ep, mask))  29.5 us
    ppermute x18, waiting for transfers between devices, move(): return lax.ppermute(value, 'ep', xor_pairs(ep, mask))  15.9 us
    all_to_all x1, blocking collectives, fast_shards(): lax.all_to_all(outgoing, 'ep', split_axis=0, concat_axis=0, tiled=True)  12.4 us
    pallas_call x10, Pallas kernels, call(): pl.pallas_call(kernel, out_shape=outs, in_specs=[pl.BlockSpec(memory_spac...  6.84 us
    all_to_all x1, starting transfers between devices, fast_shards(): lax.all_to_all(reduced.reshape(ep, rows_out, part), 'ep', split_axis=0, c...  3.52 us
    ppermute x3, waiting for transfers between devices, swap(): return lax.ppermute(value, 'tp', [(0, 1), (1, 0)])  2.55 us
    unnamed x28, local copies, waits for them, and re-layouts  2.4 us
    pallas_call x1, Pallas kernels, fast_shards(): pl.pallas_call(update_kernel, out_shape=shaped(*state.shape, dtype=f32),...  2.36 us
  transfers between devices with their start and end apart: 22, of which 10 were waited for; matrix products, arithmetic and copies ran while one was open for 0% of the time, Pallas kernels for 7%

commit v1 on v0

--- a/solution.py
+++ b/solution.py
@@ -88,7 +88,10 @@
         copy.wait()
 
 
-def route_kernel(cap, span, ids_ref, weights_ref, info_ref, combine_ref, matrix_ref):
+def route_kernel(cap, span, ids_ref, weights_ref, tokens_ref, info_ref, combine_ref, matrix_ref, scale_ref):
+    tokens = tokens_ref[...].astype(jnp.float32)
+    scale = lax.rsqrt(jnp.mean(tokens * tokens, axis=-1, keepdims=True) + epsilon)
+    scale_ref[...] = jnp.broadcast_to(scale, scale_ref.shape)
     matrix_ref[...] = spreader(ids_ref.shape[0])
     count = ids_ref.shape[0]
     ids, weights = ids_ref[...], weights_ref[...]
@@ -138,15 +141,14 @@
 
 def readout_kernel(group, outer, *refs):
     part_refs = refs[:group]
-    tokens_ref, bound_ref, gain_ref, info_ref, matrix_ref, state_ref = refs[group : group + 6]
-    forget_ref, fresh_ref = refs[group + 6 : group + 8]
-    payloads = refs[group + 8 :]
+    tokens_ref, bound_ref, gain_ref, info_ref, matrix_ref, scale_ref, state_ref = refs[group : group + 7]
+    forget_ref, fresh_ref = refs[group + 7 : group + 9]
+    payloads = refs[group + 9 :]
     count = tokens_ref.shape[0]
     proj = bound_ref.shape[1]
     half = outer // 2
 
-    tokens = tokens_ref[...].astype(jnp.float32)
-    scale = lax.rsqrt(jnp.mean(tokens * tokens, axis=-1, keepdims=True) + epsilon)
+    scale = scale_ref[...]
     matrix = matrix_ref[...]
     for head in range(proj // LANES):
 
@@ -400,10 +402,10 @@
 
     cap = 3 * count // 8
     rows_out = GROUP * cap
-    info, combine, matrix = call(
+    info, combine, matrix, scale = call(
         functools.partial(route_kernel, cap, span),
-        (route_ids, route_weights),
-        [shaped(count, LANES), shaped(count, ep * rows_out, dtype=f32), shaped(3 * count, count * LANES)],
+        (route_ids, route_weights, tokens),
+        [shaped(count, LANES), shaped(count, ep * rows_out, dtype=f32), shaped(3 * count, count * LANES), shaped(count, LANES, dtype=f32)],
     )
 
     parts = call(
@@ -421,6 +423,7 @@
         head_gain.reshape(1, proj),
         info,
         matrix,
+        scale,
         state,
     )
     forget, fresh, *payloads = call(

time: 78.4 us -> 78.3 us (level)
  no operation moved by 1% of the time
where the time goes in v1:
time: 78.3 us; the launch traced here: 78 us
  starting transfers between devices  33.2 us (42%)
  waiting for transfers between devices  19.2 us (25%)
  blocking collectives  12.5 us (16%)
  Pallas kernels  9.11 us (12%)
  local copies, waits for them, and re-layouts  2.4 us (3%)
  between operations  0.85 us (1%)
    ppermute x18, starting transfers between devices, move(): return lax.ppermute(value, 'ep', xor_pairs(ep, mask))  29.4 us
    ppermute x18, waiting for transfers between devices, move(): return lax.ppermute(value, 'ep', xor_pairs(ep, mask))  15.9 us
    all_to_all x1, blocking collectives, fast_shards(): lax.all_to_all(outgoing, 'ep', split_axis=0, concat_axis=0, tiled=True)  12.5 us
    pallas_call x10, Pallas kernels, call(): pl.pallas_call(kernel, out_shape=outs, in_specs=[pl.BlockSpec(memory_spac...  6.74 us
    all_to_all x1, starting transfers between devices, fast_shards(): lax.all_to_all(reduced.reshape(ep, rows_out, part), 'ep', split_axis=0, c...  3.52 us
    ppermute x3, waiting for transfers between devices, swap(): return lax.ppermute(value, 'tp', [(0, 1), (1, 0)])  2.55 us
    unnamed x28, local copies, waits for them, and re-layouts  2.4 us
    pallas_call x1, Pallas kernels, fast_shards(): pl.pallas_call(update_kernel, out_shape=shaped(*state.shape, dtype=f32),...  2.37 us
  transfers between devices with their start and end apart: 22, of which 10 were waited for; matrix products, arithmetic and copies ran while one was open for 0% of the time, Pallas kernels for 7%

profile of v1, /device:TPU:0, one launch (start us, length us, event | category | flops | bytes accessed | tf_op | source)
XLA Modules:
  0.0 78.0 jit_solution(16828950259996862564)
XLA Ops:
  0.6 0.0 copy-start.11
  0.6 0.0 copy-start.12
  0.7 0.0 copy-start.6
  0.7 1.3 %shard_map.158 = (bf16[128,1536]{1,0:T(8,128)(2,1)S(1)}, bf16[16,512]{1,0:T(8,128)(2,1)S(1)}, bf16[16,512]{1,0:T(8,128)(2,1)S(1)}, bf16[16,512]{1,0:T(8,128)(2,1)S(1)}, bf16[16,512]{1,0:T(8,128)(2,1)S(1)}) custom-call(bf16[16,2048]{1,0:T(8,128)(2,1)} %refs_4_.2, bf16[128,512]{1,0:T(8,128)(2,1)} %refs_0_.1, bf16[128,512]{1,0:T(8,128)(2,1)} %refs_1_.1, ...), custom_call_target="tpu_custom_call" | custom-call | flops 3000000000 | bytes 100000 | tf_op jit(solution)/shard_map/pallas_call | solution.py:32
  1.9 3.1 %collective-permute-start.5 = (bf16[128,1536]{1,0:T(8,128)(2,1)S(1)}, bf16[128,1536]{1,0:T(8,128)(2,1)S(1)}, u32[]{:S(2)}, u32[]{:S(2)}) collective-permute-start(bf16[128,1536]{1,0:T(8,128)(2,1)S(1)} %get-tuple-element.39.refs_5_), channel_id=1, source_target_pairs={{0,8},{2,10},{4,12},{6,14},{8,0},{10,2},{12,4},{14,6},{16,24},{18,... | collective-permute-start | bytes 1179656 | tf_op jit(solution)/shard_map/ppermute | solution.py:384
  5.1 1.5 %collective-permute-start.4 = (bf16[128,1536]{1,0:T(8,128)(2,1)S(1)}, bf16[128,1536]{1,0:T(8,128)(2,1)S(1)}, u32[]{:S(2)}, u32[]{:S(2)}) collective-permute-start(bf16[128,1536]{1,0:T(8,128)(2,1)S(1)} %get-tuple-element.39.refs_5_), channel_id=1, source_target_pairs={{0,4},{2,6},{4,0},{6,2},{8,12},{10,14},{12,8},{14,10},{16,20},{18,... | collective-permute-start | bytes 1179656 | tf_op jit(solution)/shard_map/ppermute | solution.py:384
  6.6 1.5 %collective-permute-start.3 = (bf16[128,1536]{1,0:T(8,128)(2,1)S(1)}, bf16[128,1536]{1,0:T(8,128)(2,1)S(1)}, u32[]{:S(2)}, u32[]{:S(2)}) collective-permute-start(bf16[128,1536]{1,0:T(8,128)(2,1)S(1)} %get-tuple-element.39.refs_5_), channel_id=1, source_target_pairs={{0,2},{2,0},{4,6},{6,4},{8,10},{10,8},{12,14},{14,12},{16,18},{18,... | collective-permute-start | bytes 1179656 | tf_op jit(solution)/shard_map/ppermute | solution.py:384
  8.1 0.0 collective-permute-start
  8.1 2.9 %collective-permute-start.1 = (bf16[16,512]{1,0:T(8,128)(2,1)S(1)}, bf16[16,512]{1,0:T(8,128)(2,1)S(1)}, u32[]{:S(2)}, u32[]{:S(2)}) collective-permute-start(bf16[16,512]{1,0:T(8,128)(2,1)S(1)} %get-tuple-element.37), channel_id=1, source_target_pairs={{0,16},{2,18},{4,20},{6,22},{8,24},{10,26},{12,28},{14,30},{16,0},... | collective-permute-start | bytes 49160 | tf_op jit(solution)/shard_map/ppermute | solution.py:384
  11.0 6.0 %collective-permute-done.refs_1_ = bf16[16,512]{1,0:T(8,128)(2,1)S(1)} collective-permute-done((bf16[16,512]{1,0:T(8,128)(2,1)S(1)}, bf16[16,512]{1,0:T(8,128)(2,1)S(1)}, u32[]{:S(2)}, u32[]{:S(2)}) %collective-permute-start) | collective-permute-done | bytes 16416 | tf_op jit(solution)/shard_map/ppermute | solution.py:384
  17.0 3.5 %collective-permute-start.2 = (bf16[16,512]{1,0:T(8,128)(2,1)S(1)}, bf16[16,512]{1,0:T(8,128)(2,1)S(1)}, u32[]{:S(2)}, u32[]{:S(2)}) collective-permute-start(bf16[16,512]{1,0:T(8,128)(2,1)S(1)} %get-tuple-element.38), channel_id=1, source_target_pairs={{0,30},{2,28},{4,26},{6,24},{8,22},{10,20},{12,18},{14,16},{16,14}... | collective-permute-start | bytes 49160 | tf_op jit(solution)/shard_map/ppermute | solution.py:384
  20.6 0.1 copy.17.ids_ref
  20.6 0.1 copy.18.weights_ref
  20.7 0.0 collective-permute-done.1.refs_2_
  20.7 0.0 collective-permute-start.13
  20.8 3.9 %collective-permute-done.2.refs_3_ = bf16[16,512]{1,0:T(8,128)(2,1)S(1)} collective-permute-done((bf16[16,512]{1,0:T(8,128)(2,1)S(1)}, bf16[16,512]{1,0:T(8,128)(2,1)S(1)}, u32[]{:S(2)}, u32[]{:S(2)}) %collective-permute-start.2) | collective-permute-done | bytes 16416 | tf_op jit(solution)/shard_map/ppermute | solution.py:384
  24.6 0.8 %collective-permute-start.12 = (bf16[512,128]{1,0:T(8,128)(2,1)S(1)}, bf16[512,128]{1,0:T(8,128)(2,1)S(1)}, u32[]{:S(2)}, u32[]{:S(2)}) collective-permute-start(bf16[512,128]{1,0:T(8,128)(2,1)S(1)} %copy-done.6), channel_id=1, source_target_pairs={{0,8},{2,10},{4,12},{6,14},{8,0},{10,2},{12,4},{14,6},{16,24},{18,... | collective-permute-start | bytes 393224 | tf_op jit(solution)/shard_map/ppermute | solution.py:384
  25.5 0.0 collective-permute-done.5.refs_8_
  25.5 0.0 collective-permute-done.4.refs_7_
  25.5 0.0 collective-permute-done.3.refs_6_
  25.5 0.0 copy-start.7
  25.5 0.4 shard_map.159
  25.9 1.0 %collective-permute-start.6 = (bf16[16,1536]{1,0:T(8,128)(2,1)S(1)}, bf16[16,1536]{1,0:T(8,128)(2,1)S(1)}, u32[]{:S(2)}, u32[]{:S(2)}) collective-permute-start(bf16[16,1536]{1,0:T(8,128)(2,1)S(1)} %get-tuple-element.41), channel_id=1, source_target_pairs={{0,14},{2,12},{4,10},{6,8},{8,6},{10,4},{12,2},{14,0},{16,30},{18,... | collective-permute-start | bytes 147464 | tf_op jit(solution)/shard_map/ppermute | solution.py:384
  26.9 2.3 %collective-permute-start.7 = (bf16[16,1536]{1,0:T(8,128)(2,1)S(1)}, bf16[16,1536]{1,0:T(8,128)(2,1)S(1)}, u32[]{:S(2)}, u32[]{:S(2)}) collective-permute-start(bf16[16,1536]{1,0:T(8,128)(2,1)S(1)} %get-tuple-element.42), channel_id=1, source_target_pairs={{0,16},{2,18},{4,20},{6,22},{8,24},{10,26},{12,28},{14,30},{16,0},... | collective-permute-start | bytes 147464 | tf_op jit(solution)/shard_map/ppermute | solution.py:384
  29.2 3.3 %collective-permute-start.8 = (bf16[16,1536]{1,0:T(8,128)(2,1)S(1)}, bf16[16,1536]{1,0:T(8,128)(2,1)S(1)}, u32[]{:S(2)}, u32[]{:S(2)}) collective-permute-start(bf16[16,1536]{1,0:T(8,128)(2,1)S(1)} %get-tuple-element.43), channel_id=1, source_target_pairs={{0,30},{2,28},{4,26},{6,24},{8,22},{10,20},{12,18},{14,16},{16,14}... | collective-permute-start | bytes 147464 | tf_op jit(solution)/shard_map/ppermute | solution.py:384
  32.4 0.3 shard_map.160
  32.7 0.0 collective-permute-done.6.refs_1_
  32.7 2.4 %collective-permute-start.14 = (bf16[512,128]{1,0:T(8,128)(2,1)S(1)}, bf16[512,128]{1,0:T(8,128)(2,1)S(1)}, u32[]{:S(2)}, u32[]{:S(2)}) collective-permute-start(bf16[512,128]{1,0:T(8,128)(2,1)S(1)} %copy-done.6), channel_id=1, source_target_pairs={{0,24},{2,26},{4,28},{6,30},{8,16},{10,18},{12,20},{14,22},{16,8},... | collective-permute-start | bytes 393224 | tf_op jit(solution)/shard_map/ppermute | solution.py:384
  35.1 0.0 collective-permute-done.7.refs_2_
  35.1 1.9 %collective-permute-done.8.refs_3_ = bf16[16,1536]{1,0:T(8,128)(2,1)S(1)} collective-permute-done((bf16[16,1536]{1,0:T(8,128)(2,1)S(1)}, bf16[16,1536]{1,0:T(8,128)(2,1)S(1)}, u32[]{:S(2)}, u32[]{:S(2)}) %collective-permute-start.8) | collective-permute-done | bytes 49184 | tf_op jit(solution)/shard_map/ppermute | solution.py:384
  37.0 0.9 %shard_map.161 = (f32[16,512]{1,0:T(8,128)S(1)}, f32[16,512]{1,0:T(8,128)S(1)}, bf16[16,896]{1,0:T(8,128)(2,1)S(1)}, bf16[16,896]{1,0:T(8,128)(2,1)S(1)}, bf16[1...) custom-call(bf16[16,1536]{1,0:T(8,128)(2,1)S(1)} %get-tuple-element.40.refs_0_, ...), custom_call_target="tpu_custom_call" | custom-call | flops 3000000000 | bytes 100000 | tf_op jit(solution)/shard_map/pallas_call | solution.py:32
  37.8 1.4 %collective-permute-start.9 = (bf16[16,896]{1,0:T(8,128)(2,1)S(1)}, bf16[16,896]{1,0:T(8,128)(2,1)S(1)}, u32[]{:S(2)}, u32[]{:S(2)}) collective-permute-start(bf16[16,896]{1,0:T(8,128)(2,1)S(1)} %get-tuple-element.48), channel_id=1, source_target_pairs={{0,2},{2,0},{4,6},{6,4},{8,10},{10,8},{12,14},{14,12},{16,18},{18,... | collective-permute-start | bytes 86024 | tf_op jit(solution)/shard_map/ppermute | solution.py:384
  39.2 1.5 %collective-permute-start.10 = (bf16[16,896]{1,0:T(8,128)(2,1)S(1)}, bf16[16,896]{1,0:T(8,128)(2,1)S(1)}, u32[]{:S(2)}, u32[]{:S(2)}) collective-permute-start(bf16[16,896]{1,0:T(8,128)(2,1)S(1)} %get-tuple-element.49), channel_id=1, source_target_pairs={{0,4},{2,6},{4,0},{6,2},{8,12},{10,14},{12,8},{14,10},{16,20},{18,... | collective-permute-start | bytes 86024 | tf_op jit(solution)/shard_map/ppermute | solution.py:384
  40.7 0.0 collective-permute-done.13.refs_6_
  40.7 0.6 collective-permute-start.11
  41.3 0.0 collective-permute-done.12.refs_5_
  41.3 0.0 collective-permute-done.14.refs_7_
  41.3 0.4 collective-permute-done.9.refs_1_
  41.7 1.4 %collective-permute-done.10.refs_2_ = bf16[16,896]{1,0:T(8,128)(2,1)S(1)} collective-permute-done((bf16[16,896]{1,0:T(8,128)(2,1)S(1)}, bf16[16,896]{1,0:T(8,128)(2,1)S(1)}, u32[]{:S(2)}, u32[]{:S(2)}) %collective-permute-start.10) | collective-permute-done | bytes 28704 | tf_op jit(solution)/shard_map/ppermute | solution.py:384
  43.1 2.4 %collective-permute-done.11.refs_3_ = bf16[16,896]{1,0:T(8,128)(2,1)S(1)} collective-permute-done((bf16[16,896]{1,0:T(8,128)(2,1)S(1)}, bf16[16,896]{1,0:T(8,128)(2,1)S(1)}, u32[]{:S(2)}, u32[]{:S(2)}) %collective-permute-start.11) | collective-permute-done | bytes 28704 | tf_op jit(solution)/shard_map/ppermute | solution.py:384
  45.5 0.2 shard_map.162
  45.7 0.1 collective-permute-start.15
  45.8 1.2 %collective-permute-done.15.got_ref = bf16[64,256]{1,0:T(8,128)(2,1)S(1)} collective-permute-done((bf16[64,256]{1,0:T(8,128)(2,1)S(1)}, bf16[64,256]{1,0:T(8,128)(2,1)S(1)}, u32[]{:S(2)}, u32[]{:S(2)}) %collective-permute-start.15) | collective-permute-done | bytes 32800 | tf_op jit(solution)/shard_map/ppermute | solution.py:387
  47.0 0.2 shard_map.163
  47.2 12.5 %all_to_all.10.mine_ref = bf16[16,24,256]{2,1,0:T(8,128)(2,1)S(1)} all-to-all(bf16[16,24,256]{2,1,0:T(8,128)(2,1)S(1)} %get-tuple-element.55), channel_id=1, replica_groups=mesh['ep'=16,'tp'=2] {'ep'}, dimensions={0} | all-to-all | bytes 393216 | tf_op jit(solution)/shard_map/all_to_all | solution.py:463
  59.7 0.0 collective-permute-start.16
  59.7 0.8 %shard_map.164 = (f32[96,128]{1,0:T(8,128)S(1)}, f32[96,1024]{1,0:T(8,128)S(1)}, f32[96,1024]{1,0:T(8,128)S(1)}) custom-call(bf16[16,24,256]{2,1,0:T(8,128)(2,1)S(1)} %all_to_all.10.mine_ref, f32[1,2048]{1,0:T(1,128)S(1)} %bitcast.7, bf16[1,2048,1024]{2,1,0:T(8,128)(2,1)S(1)} %copy-done, bf16[1,2048,1024]{2,1,0:T(8,128)(2,1)S(1)} %copy-done.1, ...), custom_call_target="tpu_custom_call" | custom-call | flops 100000000 | bytes 100000 | tf_op jit(solution)/shard_map/pallas_call | solution.py:32
  60.6 0.6 collective-permute-done.16.theirs_ref
  61.1 1.3 %shard_map.165 = (bf16[96,1024]{1,0:T(8,128)(2,1)S(1)}, bf16[384,256]{1,0:T(8,128)(2,1)S(1)}) custom-call(bf16[16,24,256]{2,1,0:T(8,128)(2,1)S(1)} %collective-permute-done.16.theirs_ref, f32[1,2048]{1,0:T(1,128)S(1)} %bitcast.8, bf16[1,2048,1024]{2,1,0:T(8,128)(2,1)S(1)} %copy-done, bf16[1,2048,1024]{2,1,0:T(8,128)(2,1)S(1)} %copy-done.1, ...), custom_call_target="tpu_custom_call" | custom-call | flops 3000000000 | bytes 100000 | tf_op jit(solution)/shard_map/pallas_call | solution.py:32
  62.5 0.2 collective-permute-start.17
  62.7 0.5 shard_map.166
  63.2 0.8 collective-permute-done.17
  64.0 0.7 add_convert_fusion
  64.7 3.5 %all-to-all-start.1 = ((bf16[16,24,256]{2,1,0:T(8,128)(2,1)}), bf16[16,24,256]{2,1,0:T(8,128)(2,1)S(1)}, u32[]{:S(2)}, u32[]{:S(2)}) async-start(bf16[16,24,256]{2,1,0:T(8,128)(2,1)} %bitcast.4), calls=%async_computation.1 | async-start | bytes 393216 | tf_op jit(solution)/shard_map/all_to_all | solution.py:501
  68.2 1.8 %collective-permute-start.18 = (bf16[16,256]{1,0:T(8,128)(2,1)S(1)}, bf16[16,256]{1,0:T(8,128)(2,1)S(1)}, u32[]{:S(2)}, u32[]{:S(2)}) collective-permute-start(bf16[16,256]{1,0:T(8,128)(2,1)S(1)} %get-tuple-element.63), channel_id=1, source_target_pairs={{0,2},{2,0},{4,6},{6,4},{8,10},{10,8},{12,14},{14,12},{16,18},{18,... | collective-permute-start | bytes 24584 | tf_op jit(solution)/shard_map/ppermute | solution.py:384
  70.0 1.5 %collective-permute-start.19 = (bf16[16,256]{1,0:T(8,128)(2,1)S(1)}, bf16[16,256]{1,0:T(8,128)(2,1)S(1)}, u32[]{:S(2)}, u32[]{:S(2)}) collective-permute-start(bf16[16,256]{1,0:T(8,128)(2,1)S(1)} %get-tuple-element.64), channel_id=1, source_target_pairs={{0,4},{2,6},{4,0},{6,2},{8,12},{10,14},{12,8},{14,10},{16,20},{18,... | collective-permute-start | bytes 24584 | tf_op jit(solution)/shard_map/ppermute | solution.py:384
  71.5 0.3 collective-permute-start.20
  71.8 2.2 %copy-done.4 = f32[16,4,128,128]{3,2,1,0:T(8,128)S(1)} copy-done((f32[16,4,128,128]{3,2,1,0:T(8,128)S(1)}, f32[16,4,128,128]{3,2,1,0:T(8,128)}, u32[]{:S(2)}) %copy-start.4) | copy-done | bytes 4194328
  74.0 2.4 %shard_map.168 = f32[16,4,128,128]{3,2,1,0:T(8,128)} custom-call(f32[16,512]{1,0:T(8,128)S(1)} %get-tuple-element.66.forget_ref, f32[16,512]{1,0:T(8,128)S(1)} %get-tuple-element.67.fresh_ref, bf16[48,2048]{1,0:T(8,128)(2,1)S(1)} %get-tuple-element.45.refs_8_.matrix_ref, f32[16,4,128,128]{3,2,1,0:T(8,128)S(1)} %copy-done.4), custom_call_target="tpu_custom_call" | custom-call | flops 1000000000 | bytes 100000 | tf_op jit(solution)/shard_map/pallas_call | solution.py:436
  76.3 0.0 collective-permute-done.18.refs_1_
  76.4 0.0 collective-permute-done.19.refs_2_
  76.4 0.0 collective-permute-done.20.refs_3_
  76.4 0.7 all-to-all-done.1
  77.1 0.9 %shard_map.167 = bf16[16,1024]{1,0:T(8,128)(2,1)} custom-call(bf16[384,256]{1,0:T(8,128)(2,1)S(1)} %bitcast.6, f32[16,384]{1,0:T(8,128)S(1)} %get-tuple-element.61.weight_ref, bf16[16,256]{1,0:T(8,128)(2,1)S(1)} %get-tuple-element.62.refs_0_, bf16[16,256]{1,0:T(8,128)(2,1)S(1)} %collective-permute-done.18.refs_1_, ...), custom_call_target="tpu_custom_call" | custom-call | flops 3000000000 | bytes 100000 | tf_op jit(solution)/shard_map/pallas_call | solution.py:32
  (21 shorter events, 0.0 us)
Async XLA Ops:
  0.6 19.9 %copy-start.11 = (s32[16,2]{0,1:T(2,128)S(1)}, s32[16,2]{0,1:T(2,128)}, u32[]{:S(2)}) copy-start(s32[16,2]{0,1:T(2,128)} %param.25) | copy-start | bytes 388
  0.6 20.0 %copy-start.12 = (f32[16,2]{0,1:T(2,128)S(1)}, f32[16,2]{0,1:T(2,128)}, u32[]{:S(2)}) copy-start(f32[16,2]{0,1:T(2,128)} %param.26) | copy-start | bytes 388
  0.7 20.1 %copy-start.6 = (bf16[512,128]{1,0:T(8,128)(2,1)S(1)}, bf16[512,128]{1,0:T(8,128)(2,1)}, u32[]{:S(2)}) copy-start(bf16[512,128]{1,0:T(8,128)(2,1)} %refs_4_.3) | copy-start | bytes 393220
  0.7 24.8 %copy-start.8 = (f32[2048]{0:T(1024)S(1)}, f32[2048]{0:T(1024)}, u32[]{:S(2)}) copy-start(f32[2048]{0:T(1024)} %param.16) | copy-start | bytes 24580
  1.9 23.5 %collective-permute-start.5 = (bf16[128,1536]{1,0:T(8,128)(2,1)S(1)}, bf16[128,1536]{1,0:T(8,128)(2,1)S(1)}, u32[]{:S(2)}, u32[]{:S(2)}) collective-permute-start(bf16[128,1536]{1,0:T(8,128)(2,1)S(1)} %get-tuple-element.39.refs_5_), channel_id=1, source_target_pairs={{0,8},{2,10},{4,12},{6,14},{8,0},{10,2},{12,4},{14,6},{16,24},{18,... | collective-permute-start | bytes 1179656 | tf_op jit(solution)/shard_map/ppermute | solution.py:384
  5.1 20.4 %collective-permute-start.4 = (bf16[128,1536]{1,0:T(8,128)(2,1)S(1)}, bf16[128,1536]{1,0:T(8,128)(2,1)S(1)}, u32[]{:S(2)}, u32[]{:S(2)}) collective-permute-start(bf16[128,1536]{1,0:T(8,128)(2,1)S(1)} %get-tuple-element.39.refs_5_), channel_id=1, source_target_pairs={{0,4},{2,6},{4,0},{6,2},{8,12},{10,14},{12,8},{14,10},{16,20},{18,... | collective-permute-start | bytes 1179656 | tf_op jit(solution)/shard_map/ppermute | solution.py:384
  6.6 18.9 %collective-permute-start.3 = (bf16[128,1536]{1,0:T(8,128)(2,1)S(1)}, bf16[128,1536]{1,0:T(8,128)(2,1)S(1)}, u32[]{:S(2)}, u32[]{:S(2)}) collective-permute-start(bf16[128,1536]{1,0:T(8,128)(2,1)S(1)} %get-tuple-element.39.refs_5_), channel_id=1, source_target_pairs={{0,2},{2,0},{4,6},{6,4},{8,10},{10,8},{12,14},{14,12},{16,18},{18,... | collective-permute-start | bytes 1179656 | tf_op jit(solution)/shard_map/ppermute | solution.py:384
  8.1 9.0 %collective-permute-start = (bf16[16,512]{1,0:T(8,128)(2,1)S(1)}, bf16[16,512]{1,0:T(8,128)(2,1)S(1)}, u32[]{:S(2)}, u32[]{:S(2)}) collective-permute-start(bf16[16,512]{1,0:T(8,128)(2,1)S(1)} %get-tuple-element.36), channel_id=1, source_target_pairs={{0,14},{2,12},{4,10},{6,8},{8,6},{10,4},{12,2},{14,0},{16,30},{18,... | collective-permute-start | bytes 49160 | tf_op jit(solution)/shard_map/ppermute | solution.py:384
  8.1 12.6 %collective-permute-start.1 = (bf16[16,512]{1,0:T(8,128)(2,1)S(1)}, bf16[16,512]{1,0:T(8,128)(2,1)S(1)}, u32[]{:S(2)}, u32[]{:S(2)}) collective-permute-start(bf16[16,512]{1,0:T(8,128)(2,1)S(1)} %get-tuple-element.37), channel_id=1, source_target_pairs={{0,16},{2,18},{4,20},{6,22},{8,24},{10,26},{12,28},{14,30},{16,0},... | collective-permute-start | bytes 49160 | tf_op jit(solution)/shard_map/ppermute | solution.py:384
  17.0 7.6 %collective-permute-start.2 = (bf16[16,512]{1,0:T(8,128)(2,1)S(1)}, bf16[16,512]{1,0:T(8,128)(2,1)S(1)}, u32[]{:S(2)}, u32[]{:S(2)}) collective-permute-start(bf16[16,512]{1,0:T(8,128)(2,1)S(1)} %get-tuple-element.38), channel_id=1, source_target_pairs={{0,30},{2,28},{4,26},{6,24},{8,22},{10,20},{12,18},{14,16},{16,14}... | collective-permute-start | bytes 49160 | tf_op jit(solution)/shard_map/ppermute | solution.py:384
  20.7 20.0 %collective-permute-start.13 = (bf16[512,128]{1,0:T(8,128)(2,1)S(1)}, bf16[512,128]{1,0:T(8,128)(2,1)S(1)}, u32[]{:S(2)}, u32[]{:S(2)}) collective-permute-start(bf16[512,128]{1,0:T(8,128)(2,1)S(1)} %copy-done.6), channel_id=1, source_target_pairs={{0,16},{2,18},{4,20},{6,22},{8,24},{10,26},{12,28},{14,30},{16,0},... | collective-permute-start | bytes 393224 | tf_op jit(solution)/shard_map/ppermute | solution.py:384
  24.6 16.7 %collective-permute-start.12 = (bf16[512,128]{1,0:T(8,128)(2,1)S(1)}, bf16[512,128]{1,0:T(8,128)(2,1)S(1)}, u32[]{:S(2)}, u32[]{:S(2)}) collective-permute-start(bf16[512,128]{1,0:T(8,128)(2,1)S(1)} %copy-done.6), channel_id=1, source_target_pairs={{0,8},{2,10},{4,12},{6,14},{8,0},{10,2},{12,4},{14,6},{16,24},{18,... | collective-permute-start | bytes 393224 | tf_op jit(solution)/shard_map/ppermute | solution.py:384
  25.5 6.9 %copy-start.7 = (bf16[16,2048]{1,0:T(8,128)(2,1)S(1)}, bf16[16,2048]{1,0:T(8,128)(2,1)}, u32[]{:S(2)}) copy-start(bf16[16,2048]{1,0:T(8,128)(2,1)} %refs_4_.2) | copy-start | bytes 196612
  25.9 6.8 %collective-permute-start.6 = (bf16[16,1536]{1,0:T(8,128)(2,1)S(1)}, bf16[16,1536]{1,0:T(8,128)(2,1)S(1)}, u32[]{:S(2)}, u32[]{:S(2)}) collective-permute-start(bf16[16,1536]{1,0:T(8,128)(2,1)S(1)} %get-tuple-element.41), channel_id=1, source_target_pairs={{0,14},{2,12},{4,10},{6,8},{8,6},{10,4},{12,2},{14,0},{16,30},{18,... | collective-permute-start | bytes 147464 | tf_op jit(solution)/shard_map/ppermute | solution.py:384
  26.9 8.2 %collective-permute-start.7 = (bf16[16,1536]{1,0:T(8,128)(2,1)S(1)}, bf16[16,1536]{1,0:T(8,128)(2,1)S(1)}, u32[]{:S(2)}, u32[]{:S(2)}) collective-permute-start(bf16[16,1536]{1,0:T(8,128)(2,1)S(1)} %get-tuple-element.42), channel_id=1, source_target_pairs={{0,16},{2,18},{4,20},{6,22},{8,24},{10,26},{12,28},{14,30},{16,0},... | collective-permute-start | bytes 147464 | tf_op jit(solution)/shard_map/ppermute | solution.py:384
  29.1 7.8 %copy-start.3 = (f32[16,4,128,128]{3,2,1,0:T(8,128)S(1)}, f32[16,4,128,128]{3,2,1,0:T(8,128)}, u32[]{:S(2)}) copy-start(f32[16,4,128,128]{3,2,1,0:T(8,128)} %state_ref.1) | copy-start | bytes 12582916
  29.1 7.8 %copy-start.9 = (f32[512]{0:T(512)S(1)}, f32[512]{0:T(512)}, u32[]{:S(2)}) copy-start(f32[512]{0:T(512)} %param.20) | copy-start | bytes 6148
  29.1 7.8 %copy-start.10 = (f32[512]{0:T(512)S(1)}, f32[512]{0:T(512)}, u32[]{:S(2)}) copy-start(f32[512]{0:T(512)} %param.21) | copy-start | bytes 6148
  29.2 7.8 %collective-permute-start.8 = (bf16[16,1536]{1,0:T(8,128)(2,1)S(1)}, bf16[16,1536]{1,0:T(8,128)(2,1)S(1)}, u32[]{:S(2)}, u32[]{:S(2)}) collective-permute-start(bf16[16,1536]{1,0:T(8,128)(2,1)S(1)} %get-tuple-element.43), channel_id=1, source_target_pairs={{0,30},{2,28},{4,26},{6,24},{8,22},{10,20},{12,18},{14,16},{16,14}... | collective-permute-start | bytes 147464 | tf_op jit(solution)/shard_map/ppermute | solution.py:384
  32.7 8.6 %collective-permute-start.14 = (bf16[512,128]{1,0:T(8,128)(2,1)S(1)}, bf16[512,128]{1,0:T(8,128)(2,1)S(1)}, u32[]{:S(2)}, u32[]{:S(2)}) collective-permute-start(bf16[512,128]{1,0:T(8,128)(2,1)S(1)} %copy-done.6), channel_id=1, source_target_pairs={{0,24},{2,26},{4,28},{6,30},{8,16},{10,18},{12,20},{14,22},{16,8},... | collective-permute-start | bytes 393224 | tf_op jit(solution)/shard_map/ppermute | solution.py:384
  37.8 3.9 %collective-permute-start.9 = (bf16[16,896]{1,0:T(8,128)(2,1)S(1)}, bf16[16,896]{1,0:T(8,128)(2,1)S(1)}, u32[]{:S(2)}, u32[]{:S(2)}) collective-permute-start(bf16[16,896]{1,0:T(8,128)(2,1)S(1)} %get-tuple-element.48), channel_id=1, source_target_pairs={{0,2},{2,0},{4,6},{6,4},{8,10},{10,8},{12,14},{14,12},{16,18},{18,... | collective-permute-start | bytes 86024 | tf_op jit(solution)/shard_map/ppermute | solution.py:384
  39.2 3.9 %collective-permute-start.10 = (bf16[16,896]{1,0:T(8,128)(2,1)S(1)}, bf16[16,896]{1,0:T(8,128)(2,1)S(1)}, u32[]{:S(2)}, u32[]{:S(2)}) collective-permute-start(bf16[16,896]{1,0:T(8,128)(2,1)S(1)} %get-tuple-element.49), channel_id=1, source_target_pairs={{0,4},{2,6},{4,0},{6,2},{8,12},{10,14},{12,8},{14,10},{16,20},{18,... | collective-permute-start | bytes 86024 | tf_op jit(solution)/shard_map/ppermute | solution.py:384
  40.7 4.8 %collective-permute-start.11 = (bf16[16,896]{1,0:T(8,128)(2,1)S(1)}, bf16[16,896]{1,0:T(8,128)(2,1)S(1)}, u32[]{:S(2)}, u32[]{:S(2)}) collective-permute-start(bf16[16,896]{1,0:T(8,128)(2,1)S(1)} %get-tuple-element.50), channel_id=1, source_target_pairs={{0,6},{2,4},{4,2},{6,0},{8,14},{10,12},{12,10},{14,8},{16,22},{18,... | collective-permute-start | bytes 86024 | tf_op jit(solution)/shard_map/ppermute | solution.py:384
  45.5 14.2 %copy-start.2 = (bf16[1,1024,2048]{2,1,0:T(8,128)(2,1)S(1)}, bf16[1,1024,2048]{2,1,0:T(8,128)(2,1)}, u32[]{:S(2)}) copy-start(bf16[1,1024,2048]{2,1,0:T(8,128)(2,1)} %down_ref.3) | copy-start | bytes 12582916
  45.7 1.3 %collective-permute-start.15 = (bf16[64,256]{1,0:T(8,128)(2,1)S(1)}, bf16[64,256]{1,0:T(8,128)(2,1)S(1)}, u32[]{:S(2)}, u32[]{:S(2)}) collective-permute-start(bf16[64,256]{1,0:T(8,128)(2,1)S(1)} %get-tuple-element.52), channel_id=1, source_target_pairs={{0,1},{1,0},{2,3},{3,2},{4,5},{5,4},{6,7},{7,6},{8,9},{9,8},{10,11... | collective-permute-start | bytes 98312 | tf_op jit(solution)/shard_map/ppermute | solution.py:387
  47.0 12.7 %copy-start = (bf16[1,2048,1024]{2,1,0:T(8,128)(2,1)S(1)}, bf16[1,2048,1024]{2,1,0:T(8,128)(2,1)}, u32[]{:S(2)}) copy-start(bf16[1,2048,1024]{2,1,0:T(8,128)(2,1)} %gate_ref.3) | copy-start | bytes 12582916
  47.0 12.7 %copy-start.1 = (bf16[1,2048,1024]{2,1,0:T(8,128)(2,1)S(1)}, bf16[1,2048,1024]{2,1,0:T(8,128)(2,1)}, u32[]{:S(2)}) copy-start(bf16[1,2048,1024]{2,1,0:T(8,128)(2,1)} %up_ref.3) | copy-start | bytes 12582916
  47.0 12.7 %copy-start.5 = (f32[2048]{0:T(1024)S(1)}, f32[2048]{0:T(1024)}, u32[]{:S(2)}) copy-start(f32[2048]{0:T(1024)} %param.24) | copy-start | bytes 24580
  59.7 1.4 %collective-permute-start.16 = (bf16[16,24,256]{2,1,0:T(8,128)(2,1)S(1)}, bf16[16,24,256]{2,1,0:T(8,128)(2,1)S(1)}, u32[]{:S(2)}, u32[]{:S(2)}) collective-permute-start(bf16[16,24,256]{2,1,0:T(8,128)(2,1)S(1)} %all_to_all.10.mine_ref), channel_id=1, source_target_pairs={{0,1},{1,0},{2,3},{3,2},{4,5},{5,4},{6,7},{7,6},{8,9},{9,8},{10,11... | collective-permute-start | bytes 589832 | tf_op jit(solution)/shard_map/ppermute | solution.py:387
  62.5 1.5 %collective-permute-start.17 = (bf16[384,256]{1,0:T(8,128)(2,1)S(1)}, bf16[384,256]{1,0:T(8,128)(2,1)S(1)}, u32[]{:S(2)}, u32[]{:S(2)}) collective-permute-start(bf16[384,256]{1,0:T(8,128)(2,1)S(1)} %get-tuple-element.60), channel_id=1, source_target_pairs={{0,1},{1,0},{2,3},{3,2},{4,5},{5,4},{6,7},{7,6},{8,9},{9,8},{10,11... | collective-permute-start | bytes 589832 | tf_op jit(solution)/shard_map/ppermute | solution.py:387
  64.7 12.4 %all-to-all-start.1 = ((bf16[16,24,256]{2,1,0:T(8,128)(2,1)}), bf16[16,24,256]{2,1,0:T(8,128)(2,1)S(1)}, u32[]{:S(2)}, u32[]{:S(2)}) async-start(bf16[16,24,256]{2,1,0:T(8,128)(2,1)} %bitcast.4), calls=%async_computation.1 | async-start | bytes 393216 | tf_op jit(solution)/shard_map/all_to_all | solution.py:501
  68.2 8.1 %collective-permute-start.18 = (bf16[16,256]{1,0:T(8,128)(2,1)S(1)}, bf16[16,256]{1,0:T(8,128)(2,1)S(1)}, u32[]{:S(2)}, u32[]{:S(2)}) collective-permute-start(bf16[16,256]{1,0:T(8,128)(2,1)S(1)} %get-tuple-element.63), channel_id=1, source_target_pairs={{0,2},{2,0},{4,6},{6,4},{8,10},{10,8},{12,14},{14,12},{16,18},{18,... | collective-permute-start | bytes 24584 | tf_op jit(solution)/shard_map/ppermute | solution.py:384
  70.0 6.3 %collective-permute-start.19 = (bf16[16,256]{1,0:T(8,128)(2,1)S(1)}, bf16[16,256]{1,0:T(8,128)(2,1)S(1)}, u32[]{:S(2)}, u32[]{:S(2)}) collective-permute-start(bf16[16,256]{1,0:T(8,128)(2,1)S(1)} %get-tuple-element.64), channel_id=1, source_target_pairs={{0,4},{2,6},{4,0},{6,2},{8,12},{10,14},{12,8},{14,10},{16,20},{18,... | collective-permute-start | bytes 24584 | tf_op jit(solution)/shard_map/ppermute | solution.py:384
  71.5 4.9 %collective-permute-start.20 = (bf16[16,256]{1,0:T(8,128)(2,1)S(1)}, bf16[16,256]{1,0:T(8,128)(2,1)S(1)}, u32[]{:S(2)}, u32[]{:S(2)}) collective-permute-start(bf16[16,256]{1,0:T(8,128)(2,1)S(1)} %get-tuple-element.65), channel_id=1, source_target_pairs={{0,6},{2,4},{4,2},{6,0},{8,14},{10,12},{12,10},{14,8},{16,22},{18,... | collective-permute-start | bytes 24584 | tf_op jit(solution)/shard_map/ppermute | solution.py:384
  71.8 2.2 %copy-start.4 = (f32[16,4,128,128]{3,2,1,0:T(8,128)S(1)}, f32[16,4,128,128]{3,2,1,0:T(8,128)}, u32[]{:S(2)}) copy-start(f32[16,4,128,128]{3,2,1,0:T(8,128)} %state_ref.1) | copy-start | bytes 12582916
